TPU v7x, 32 devices: a whole 2x2x4 slice. The times are simulated.
32 devices in a mesh: kv: 8 (over z, x), tp: 4 (over y, core).
Axes of the slice: x: 2, y: 2, z: 4, core: 2. Of those that a mesh axis runs over, the one named last changes fastest.
Arguments:
- tokens: bfloat16 [16384, 2048], P('kv'), may hold values from -6 to 6
- norm_gain: bfloat16 [2048], replicated, may hold values from 0.099609375 to 1.8984375
- query_weight: bfloat16 [2048, 1024], P(None, 'tp'), may hold values from -0.125 to 0.125
- cmp_key_weight: bfloat16 [2048, 512], P(None, 'tp'), may hold values from -0.125 to 0.125
- cmp_value_weight: bfloat16 [2048, 512], P(None, 'tp'), may hold values from -0.125 to 0.125
- sel_key_weight: bfloat16 [2048, 512], P(None, 'tp'), may hold values from -0.125 to 0.125
- sel_value_weight: bfloat16 [2048, 512], P(None, 'tp'), may hold values from -0.125 to 0.125
- branch_weight: bfloat16 [2, 2048, 16], replicated, may hold values from -0.125 to 0.125
- key_embed: bfloat16 [8, 32, 64], P('tp'), may hold values from -3 to 3
- key_inner: bfloat16 [8, 2048, 64], P('tp'), may hold values from -0.125 to 0.125
- key_outer: bfloat16 [8, 64, 64], P('tp'), may hold values from -0.75 to 0.75
- value_embed: bfloat16 [8, 32, 64], P('tp'), may hold values from -3 to 3
- value_inner: bfloat16 [8, 2048, 64], P('tp'), may hold values from -0.125 to 0.125
- value_outer: bfloat16 [8, 64, 64], P('tp'), may hold values from -0.75 to 0.75
- out_weight: bfloat16 [1024, 2048], replicated, may hold values from -0.1875 to 0.1875
- chosen: int32 [8, 128, 8], P('tp'), may hold values from 0 to 255, as said below
Outputs:
- attended: bfloat16 [16384, 2048], P(('kv', 'tp'))
Inputs may be any that keep to these rules, and one draw needn't show every extreme that they name: `chosen`: each entry is the index of a block of 64 positions in the whole sequence. For every key head and query block, its 8 entries lie in 8 different aligned spans of 2048 positions (at most one from any span), and none lies inside the query block's own positions.
All inputs are finite; a program needn't handle non-finite values.
Results may differ from a plain program's by a relative error of at most 0.0075.
Values may be sent and summed in bfloat16 or wider, within the bound.
A program may use at most 128 MiB of HBM per device.

v0:
```python
import functools

import jax
import jax.numpy as jnp
from jax import lax
from jax.experimental import pallas as pl
from jax.experimental.pallas import tpu as pltpu
from jax.sharding import PartitionSpec as P

HEAD_DIM = 64
CMP_BLOCK = 32
SEL_BLOCK = 64
Q_BLOCK = 128
FAR_PICKS = 8
LANES = 2 * HEAD_DIM
PLANES = 4
MESH = pl.DeviceIdType.MESH

ROPE_BASE = 10000.0
norm_eps = 1e-06
MASKED = -1e30

def params(n_axes, limit=48):
    return pltpu.CompilerParams(
        dimension_semantics=("arbitrary",) * n_axes, vmem_limit_bytes=limit * 1024 * 1024
    )


def norm_rows(tok_ref, gain_ref):
    x = tok_ref[...].astype(jnp.float32)
    inv = lax.rsqrt(jnp.mean(x * x, axis=-1, keepdims=True) + norm_eps)
    return (x * inv * gain_ref[...].astype(jnp.float32)).astype(jnp.bfloat16)


def turn(x, cosine, sine_up, sine_down):
    quarter = HEAD_DIM // 2
    return (
        x * cosine
        + pltpu.roll(x, LANES - quarter, 1) * sine_up
        + pltpu.roll(x, quarter, 1) * sine_down
    )


def low_lanes(shape):
    return lax.broadcasted_iota(jnp.int32, shape, 1) < HEAD_DIM


def sel_kernel(tok_ref, gain_ref, w_ref, cos_ref, up_ref, down_ref, *outs):
    normed = norm_rows(tok_ref, gain_ref)
    y = jnp.dot(normed, w_ref[...], preferred_element_type=jnp.float32)
    for k, out in enumerate(outs):
        x = y[:, k * LANES : (k + 1) * LANES]
        low = low_lanes(x.shape)
        turned = turn(x, cos_ref[...], up_ref[...], down_ref[...])
        out[...] = jnp.where(low, turned, x).astype(jnp.bfloat16)


def nt_dot(a, b):
    return lax.dot_general(a, b, (((1,), (1,)), ((), ())), preferred_element_type=jnp.float32)


def gate_lanes(gate, first, shape):
    return jnp.where(low_lanes(shape), gate[:, first : first + 1], gate[:, first + 1 : first + 2])


def merge(out, rows):
    low = low_lanes((rows, LANES))
    return jnp.where(low, pltpu.roll(out[:rows], HEAD_DIM, 1), out[rows:])


def exchange_kernel(
    planes,
    idx_ref,
    bias_ref,
    gain_ref,
    ke_ref,
    ko_ref,
    ve_ref,
    vo_ref,
    tok_hbm,
    w_hbm,
    cos_hbm,
    up_hbm,
    down_hbm,
    ki_hbm,
    vi_hbm,
    *rest,
):
    kv_local = bias_ref.shape[0]
    own_hbm, rest = rest[:kv_local], rest[kv_local:]
    out_ref, rest = rest[0], rest[1:]
    held, rest = rest[:kv_local], rest[kv_local:]
    (
        tok,
        w,
        cosine,
        up,
        down,
        ki,
        vi,
        qp,
        qt,
        ck,
        cv,
        gate,
        sums,
        oc,
        mix,
        got,
        local_sem,
        send_sem,
        recv_sem,
        sum_send,
        sum_recv,
        mix_send,
        mix_recv,
    ) = rest
    owners, ranks = sums.shape[0], got.shape[0]
    rows, width = tok.shape
    span = rows // SEL_BLOCK
    across = owners // planes
    me, rank = lax.axis_index("kv"), lax.axis_index("tp")
    z, x = me // across, me % across

    barrier = pltpu.get_barrier_semaphore()
    for d in range(1, owners):
        pl.semaphore_signal(barrier, inc=1, device_id={"kv": (me + d) % owners}, device_id_type=MESH)
    for d in range(1, ranks):
        pl.semaphore_signal(barrier, inc=1, device_id={"tp": (rank + d) % ranks}, device_id_type=MESH)
    loads = [
        (tok_hbm, tok),
        (w_hbm, w),
        (cos_hbm, cosine),
        (up_hbm, up),
        (down_hbm, down),
        (ki_hbm, ki),
        (vi_hbm, vi),
    ]
    copies = [pltpu.make_async_copy(a, b, local_sem.at[n]) for n, (a, b) in enumerate(loads)]
    for k in range(kv_local):
        copies.append(
            pltpu.make_async_copy(own_hbm[k], held[k].at[pl.ds(0, span)], local_sem.at[len(loads) + k])
        )
    for copy in copies:
        copy.start()
    pl.semaphore_wait(barrier, owners + ranks - 2)

    def slot(k, n):
        return held[k].at[pl.ds(n * span, span)]

    def hop(k, dz, dx):
        n = dz * across + dx
        if dx:
            source = own_hbm[k] if dz == 0 else slot(k, dz * across)
            target = z * across + (x + dx) % across
            sends = (x + dx < across) if dz == 0 else (z >= dz)
            gets = (x >= dx) if dz == 0 else (z >= dz)
        else:
            source = slot(k, (dz - 1) * across) if dz > 1 else own_hbm[k]
            target = lax.rem(me + across, owners)
            sends = (z >= dz - 1) & (z + 1 < planes)
            gets = z >= dz
        copy = pltpu.make_async_remote_copy(
            src_ref=source,
            dst_ref=slot(k, n),
            send_sem=send_sem.at[k, n],
            recv_sem=recv_sem.at[k, n],
            device_id={"kv": target},
            device_id_type=MESH,
        )
        return copy, sends, gets

    def send(k, dz, dx):
        copy, sends, _ = hop(k, dz, dx)
        pl.when(sends)(copy.start)

    def arrive(k, dz, dx):
        copy, _, gets = hop(k, dz, dx)
        pl.when(gets)(copy.wait_recv)

    def send_own(k):
        if planes > 1:
            send(k, 1, 0)
        for dx in range(1, across):
            send(k, 0, dx)

    def forward(k, dz):
        if dz >= planes:
            return
        arrive(k, dz, 0)
        if dz + 1 < planes:
            send(k, dz + 1, 0)
        for dx in range(1, across):
            send(k, dz, dx)

    for k in range(kv_local):
        send_own(k)
    for copy in copies:
        copy.wait()

    tile = 256
    scale = HEAD_DIM ** (-0.5)
    base = kv_local * LANES
    kv_width = kv_local * HEAD_DIM

    def project(i, carry):
        at = pl.ds(pl.multiple_of(i * tile, tile), tile)
        normed = norm_rows(tok.at[at], gain_ref)
        y = jnp.dot(normed, w[...], preferred_element_type=jnp.float32)
        for k in range(kv_local):
            v = y[:, k * LANES : (k + 1) * LANES]
            low = low_lanes(v.shape)
            turned = turn(v, cosine[at], up[at], down[at]) * scale
            for ref, q in ((qp, v * scale), (qt, turned)):
                ref[k, 0, at] = jnp.where(low, q, 0.0).astype(jnp.bfloat16)
                ref[k, 1, at] = jnp.where(low, pltpu.roll(q, HEAD_DIM, 1), 0.0).astype(jnp.bfloat16)
        ck[at] = y[:, base : base + kv_width].astype(jnp.bfloat16).astype(jnp.float32)
        cv[at] = y[:, base + kv_width : base + 2 * kv_width].astype(jnp.bfloat16).astype(jnp.float32)
        gate[at] = jax.nn.sigmoid(y[:, base + 2 * kv_width :])
        return carry

    lax.fori_loop(0, rows // tile, project, 0)

    blocks = rows // CMP_BLOCK

    def summarize(x_ref, e_ref, i_ref, o_ref):
        embed = jnp.concatenate([e_ref[k].astype(jnp.float32) for k in range(kv_local)], axis=1)
        parts = []
        for c in range(CMP_BLOCK):
            part = x_ref[pl.ds(c, blocks, stride=CMP_BLOCK), :] + embed[c : c + 1]
            parts.append(part.astype(jnp.bfloat16))
        flat = jnp.concatenate(parts, axis=1)
        hidden = jnp.dot(flat, inner_diagonal(i_ref[...]), preferred_element_type=jnp.float32)
        hidden = jax.nn.gelu(hidden).astype(jnp.bfloat16)
        return jnp.dot(hidden, block_diagonal(o_ref[...]), preferred_element_type=jnp.float32)

    sk = summarize(ck, ke_ref, ki, ko_ref)
    sv = summarize(cv, ve_ref, vi, vo_ref)
    for k in range(kv_local):
        cut = slice(k * HEAD_DIM, (k + 1) * HEAD_DIM)
        sums[me, k] = jnp.concatenate([sk[:, cut], sv[:, cut]], axis=1).astype(jnp.bfloat16)

    def sum_copy(d, source):
        return pltpu.make_async_remote_copy(
            src_ref=sums.at[source],
            dst_ref=sums.at[source],
            send_sem=sum_send.at[d],
            recv_sem=sum_recv.at[d],
            device_id={"kv": (me + d) % owners},
            device_id_type=MESH,
        )

    for d in range(1, owners):
        sum_copy(d, me).start()
    for k in range(kv_local):
        forward(k, 1)
    for d in range(1, owners):
        sum_copy(d, (me + owners - d) % owners).wait_recv()

    def compress(i, carry):
        at = pl.ds(pl.multiple_of(i * tile, tile), tile)
        row = lax.broadcasted_iota(jnp.int32, (2 * tile, 1), 0)
        pos = me * rows + i * tile + jnp.where(row >= tile, row - tile, row)
        lane = lax.broadcasted_iota(jnp.int32, (1, owners * blocks), 1)
        allowed = (lane + 1) * CMP_BLOCK - 1 <= pos
        for k in range(kv_local):
            keys = jnp.concatenate([sums[s, k] for s in range(owners)], axis=0)
            q = jnp.concatenate([qp[k, 0, at], qp[k, 1, at]], axis=0)
            s = jnp.where(allowed, nt_dot(q, keys), MASKED)
            top = jnp.max(s, axis=-1, keepdims=True)
            e = jnp.where(allowed, jnp.exp(s - top), 0.0)
            total = jnp.sum(e, axis=-1, keepdims=True)
            o = jnp.dot(e.astype(jnp.bfloat16), keys, preferred_element_type=jnp.float32)
            o = o * jnp.where(total > 0.0, 1.0 / jnp.where(total > 0.0, total, 1.0), 0.0)
            o = merge(o, tile)
            oc[k, at] = o * gate_lanes(gate[at], 2 * k, o.shape)
        return carry

    tiles = rows // tile
    bounds = [tiles * k // kv_local for k in range(kv_local + 1)]
    for k in range(kv_local):
        lax.fori_loop(bounds[k], bounds[k + 1], compress, 0)
        forward(k, 2)
    for dz in range(3, planes):
        for k in range(kv_local):
            forward(k, dz)

    rank_rows = rows // ranks
    group = rank_rows // Q_BLOCK
    q_blocks = rows // Q_BLOCK
    half_gates = 2 * kv_local

    def mix_copy(k, step):
        target = (rank + 1 + step) % ranks
        at = pl.ds(pl.multiple_of(target * rank_rows, rank_rows), rank_rows)
        return pltpu.make_async_remote_copy(
            src_ref=mix.at[k, at],
            dst_ref=got.at[rank, k],
            send_sem=mix_send.at[k, step],
            recv_sem=mix_recv.at[k, step],
            device_id={"tp": target},
            device_id_type=MESH,
        )

    def choose(k):
        def one(step, carry):
            target = (rank + 1 + step) % ranks
            for u in range(group):
                j = target * group + u
                at = pl.ds(pl.multiple_of(j * Q_BLOCK, Q_BLOCK), Q_BLOCK)
                own = j * (Q_BLOCK // SEL_BLOCK)
                parts = [held[k][own + b] for b in range(Q_BLOCK // SEL_BLOCK)]
                for a in range(FAR_PICKS):
                    pick = idx_ref[(k * q_blocks + j) * FAR_PICKS + a]
                    parts.append(held[k][pick])
                keys = jnp.concatenate(parts, axis=0)
                q = jnp.concatenate([qt[k, 0, at], qt[k, 1, at]], axis=0)
                s = nt_dot(q, keys) + bias_ref[k, j]
                row = lax.broadcasted_iota(jnp.int32, (2 * Q_BLOCK, Q_BLOCK), 0)
                row = jnp.where(row >= Q_BLOCK, row - Q_BLOCK, row)
                lane = lax.broadcasted_iota(jnp.int32, row.shape, 1)
                near = jnp.where(lane > row, MASKED, s[:, :Q_BLOCK])
                s = jnp.concatenate([near, s[:, Q_BLOCK:]], axis=1)
                top = jnp.max(s, axis=-1, keepdims=True)
                e = jnp.exp(s - top)
                total = jnp.sum(e, axis=-1, keepdims=True)
                o = jnp.dot(e.astype(jnp.bfloat16), keys, preferred_element_type=jnp.float32)
                o = merge(o * (1.0 / total), Q_BLOCK)
                g = gate_lanes(gate[at], half_gates + 2 * k, o.shape)
                mix[k, at] = (oc[k, at] + o * g).astype(jnp.bfloat16)
            pl.when(step > 0)(lambda: mix_copy(k, step - 1).start())
            return carry

        lax.fori_loop(0, ranks, one, 0)

    moves = [(dz, dx) for dz in range(planes) for dx in range(across) if (dz, dx) != (0, 0)]
    for k in range(kv_local):
        for dz, dx in moves:
            if dx:
                arrive(k, dz, dx)
        choose(k)
    own_at = pl.ds(pl.multiple_of(rank * rank_rows, rank_rows), rank_rows)
    for k in range(kv_local):
        for dz, dx in moves:
            copy, sends, _ = hop(k, dz, dx)
            pl.when(sends)(copy.wait_send)
    for d in range(1, owners):
        sum_copy(d, me).wait_send()
    for k in range(kv_local):
        got[rank, k] = mix[k, own_at]
        for step in range(ranks - 1):
            mix_copy(k, step).wait_send()
            mix_copy(k, step).wait_recv()
    for t in range(ranks):
        for k in range(kv_local):
            first = (t * kv_local + k) * LANES
            out_ref[:, first : first + LANES] = got[t, k]


def cost(flops, moved):
    return pl.CostEstimate(flops=int(flops), bytes_accessed=int(moved), transcendentals=0)


def block_diagonal(w):
    n, a, b = w.shape
    zero = jnp.zeros((a, b), w.dtype)
    return jnp.concatenate(
        [jnp.concatenate([w[i] if i == j else zero for j in range(n)], axis=1) for i in range(n)],
        axis=0,
    )


def inner_diagonal(w):
    n, _, e = w.shape
    zero = jnp.zeros((HEAD_DIM, e), w.dtype)
    parts = []
    for c in range(CMP_BLOCK):
        for i in range(n):
            cut = w[i, c * HEAD_DIM : (c + 1) * HEAD_DIM]
            parts.append(jnp.concatenate([cut if i == j else zero for j in range(n)], axis=1))
    return jnp.concatenate(parts, axis=0)


def per_device(
    tokens,
    norm_gain,
    query_weight,
    cmp_key_weight,
    cmp_value_weight,
    sel_key_weight,
    sel_value_weight,
    branch_weight,
    key_embed,
    key_inner,
    key_outer,
    value_embed,
    value_inner,
    value_outer,
    out_weight,
    chosen,
):
    rows, width = tokens.shape
    kv_local = key_embed.shape[0]
    heads_local = query_weight.shape[1] // HEAD_DIM
    owners = lax.axis_size("kv")
    me = lax.axis_index("kv")
    planes = PLANES if owners % PLANES == 0 else 1
    across = owners // planes
    my_z, my_x = me // across, me % across
    offset = me * rows
    f32 = jnp.float32
    bf16 = jnp.bfloat16

    half = HEAD_DIM // 2
    lane = jnp.arange(LANES, dtype=jnp.int32)
    inverse = ROPE_BASE ** (-(lane % half).astype(f32) / half)
    positions = offset + jnp.arange(rows, dtype=jnp.int32)
    phases = positions.astype(f32)[:, None] * inverse[None, :]
    cosine = jnp.cos(phases)
    sine = jnp.sin(phases)
    first = (lane % HEAD_DIM < half)[None, :]
    up = jnp.where(first, -sine, 0.0)
    down = jnp.where(first, 0.0, sine)
    gain = norm_gain.reshape(1, width)

    def heads_of(w, k):
        return w[:, k * HEAD_DIM : (k + 1) * HEAD_DIM]

    sel_weight = jnp.concatenate(
        [heads_of(w, k) for k in range(kv_local) for w in (sel_key_weight, sel_value_weight)],
        axis=1,
    )
    tile = 256
    steps = rows // tile
    row_spec = lambda cols: pl.BlockSpec((tile, cols), lambda i: (i, 0))
    full = lambda shape: pl.BlockSpec(shape, lambda *_: (0,) * len(shape))
    kv = pl.pallas_call(
        sel_kernel,
        grid=(steps,),
        in_specs=[row_spec(width), full((1, width)), full(sel_weight.shape)]
        + [row_spec(LANES)] * 3,
        out_specs=[row_spec(LANES)] * kv_local,
        out_shape=[jax.ShapeDtypeStruct((rows, LANES), bf16)] * kv_local,
        compiler_params=params(1),
        cost_estimate=cost(2 * rows * width * sel_weight.shape[1], rows * width * 2),
        name="sel_project",
    )(tokens, gain, sel_weight, cosine, up, down)

    gate_cols = lax.dynamic_slice_in_dim(
        branch_weight, lax.axis_index("tp") * heads_local, heads_local, 2
    )
    gate_weight = jnp.concatenate([gate_cols[0], gate_cols[1]], axis=1)
    gate_count = 2 * heads_local
    mid_weight = jnp.concatenate(
        [query_weight, cmp_key_weight, cmp_value_weight, jnp.pad(gate_weight, ((0, 0), (0, LANES - gate_count)))],
        axis=1,
    )
    kv_width = kv_local * HEAD_DIM
    blocks = rows // CMP_BLOCK
    q_blocks = rows // Q_BLOCK
    span_blocks = rows // SEL_BLOCK
    picks = lax.dynamic_slice_in_dim(chosen.astype(jnp.int32), me * q_blocks, q_blocks, 1)
    own_first = (me * q_blocks + jnp.arange(q_blocks, dtype=jnp.int32)) * (Q_BLOCK // SEL_BLOCK)
    usable = picks < own_first[None, :, None]
    span = picks // span_blocks
    slot = (my_z - span // across) * across + (my_x - span % across) % across
    index = jnp.where(usable, slot * span_blocks + picks % span_blocks, 0).reshape(-1)
    bias = jnp.where(usable, 0.0, MASKED).astype(f32)
    bias = jnp.repeat(bias, SEL_BLOCK, axis=-1)
    bias = jnp.pad(bias, ((0, 0), (0, 0), (Q_BLOCK, 0)))[:, :, None, :]

    ranks = lax.axis_size("tp")
    rank_rows = rows // ranks
    operands = (
        index,
        bias,
        gain,
        key_embed,
        key_outer,
        value_embed,
        value_outer,
        tokens,
        mid_weight,
        cosine,
        up,
        down,
        key_inner,
        value_inner,
        *[own.reshape(span_blocks, SEL_BLOCK, LANES) for own in kv],
    )
    vmem = pl.BlockSpec(memory_space=pltpu.VMEM)
    hbm = pl.BlockSpec(memory_space=pl.ANY)
    dma = pltpu.SemaphoreType.DMA
    spread = pltpu.VMEM((kv_local, 2, rows, LANES), bf16)
    gathered = pl.pallas_call(
        functools.partial(exchange_kernel, planes),
        in_specs=[pl.BlockSpec(memory_space=pltpu.SMEM)] + [vmem] * 6 + [hbm] * (7 + kv_local),
        out_specs=vmem,
        out_shape=jax.ShapeDtypeStruct((rank_rows, ranks * kv_local * LANES), bf16),
        scratch_shapes=[pltpu.VMEM((owners * span_blocks, SEL_BLOCK, LANES), bf16)] * kv_local
        + [
            pltpu.VMEM(tokens.shape, bf16),
            pltpu.VMEM(mid_weight.shape, bf16),
            pltpu.VMEM(cosine.shape, f32),
            pltpu.VMEM(cosine.shape, f32),
            pltpu.VMEM(cosine.shape, f32),
            pltpu.VMEM(key_inner.shape, bf16),
            pltpu.VMEM(value_inner.shape, bf16),
            spread,
            spread,
            pltpu.VMEM((rows, kv_width), f32),
            pltpu.VMEM((rows, kv_width), f32),
            pltpu.VMEM((rows, LANES), f32),
            pltpu.VMEM((owners, kv_local, blocks, LANES), bf16),
            pltpu.VMEM((kv_local, rows, LANES), f32),
            pltpu.VMEM((kv_local, rows, LANES), bf16),
            pltpu.VMEM((ranks, kv_local, rank_rows, LANES), bf16),
            dma((7 + kv_local,)),
            dma((kv_local, owners)),
            dma((kv_local, owners)),
            dma((owners,)),
            dma((owners,)),
            dma((kv_local, ranks)),
            dma((kv_local, ranks)),
        ],
        compiler_params=pltpu.CompilerParams(
            collective_id=0, has_side_effects=True, vmem_limit_bytes=60 * 1024 * 1024
        ),
        cost_estimate=cost(4e10, 2e7),
        name="exchange",
    )(*operands)
    return jnp.dot(gathered, out_weight, preferred_element_type=f32).astype(bf16)


def solution(mesh):
    placed = (
        P("kv", None),
        P(),
        P(None, "tp"),
        P(None, "tp"),
        P(None, "tp"),
        P(None, "tp"),
        P(None, "tp"),
        P(),
        P("tp", None, None),
        P("tp", None, None),
        P("tp", None, None),
        P("tp", None, None),
        P("tp", None, None),
        P("tp", None, None),
        P(),
        P("tp", None, None),
    )
    return jax.shard_map(
        per_device, mesh=mesh, in_specs=placed, out_specs=P(("kv", "tp"), None), check_vma=False
    )
```

profile of v0, /device:TPU:27, one launch (start us, length us, event | category | flops | bytes accessed | tf_op | source)
XLA Modules:
  0.0 145.6 jit_solution(4344219773329248390)
XLA Ops:
  0.0 0.8 broadcast_select_fusion
  0.8 0.8 fusion.10
  1.6 0.1 copy.26
  1.6 0.7 reshape.48.idx_ref
  2.3 2.0 %fusion.21 = (bf16[2048,64]{1,0:T(8,128)(2,1)S(1)}, bf16[2048,64]{1,0:T(8,128)(2,1)S(1)}, bf16[2048,64]{1,0:T(8,128)(2,1)S(1)}, bf16[2048,64]{1,0:T(8,128)(2,1)S(1)}) fusion(bf16[2048,128]{1,0:T(8,128)(2,1)} %param.21, bf16[2048,128]{1,0:T(8,128)(2,1)} %param.22), kind=kLoop, calls=%fused_computation.50 | loop fusion | bytes 2097152 | tf_op jit(solution)/shard_map/slice | solution.py:427
  4.3 0.0 copy-start.10
  4.3 0.7 pad_maximum_fusion.w_ref
  5.1 3.8 %fusion.2 = (f32[2048,128]{1,0:T(8,128)S(1)}, f32[2048,128]{1,0:T(8,128)S(1)}, f32[2048,128]{1,0:T(8,128)S(1)}) fusion(f32[128]{0:T(128)S(1)} %fusion.19, f32[2048]{0:T(1024)S(1)} %add_convert_fusion, pred[128]{0:T(512)(128)(4,1)S(1)} %fusion.20), kind=kLoop, calls=%fused_computation.6 | loop fusion | flops 1048576 | bytes 3154560 | tf_op jit(solution)/shard_map/jit(_where)/select_n | solution.py:423
  8.9 0.0 copy-start
  8.9 0.0 copy-start.1
  8.9 0.0 copy-start.2
  8.9 0.0 copy-done.10
  9.0 0.0 copy-start.3
  9.0 0.0 copy-start.6
  9.0 0.0 copy-start.7
  9.0 0.0 copy-start.8
  9.0 10.8 %sel_project.1 = (bf16[2048,128]{1,0:T(8,128)(2,1)S(1)}, bf16[2048,128]{1,0:T(8,128)(2,1)S(1)}) custom-call(bf16[2048,2048]{1,0:T(8,128)(2,1)} %tok_hbm.1, bf16[1,2048]{1,0:T(2,128)(2,1)S(1)} %reshape.50.gain_ref, bf16[2048,256]{1,0:T(8,128)(2,1)S(1)} %pad_maximum_fusion.w_ref, f32[2048,128]{1,0:T(8,128)S(1)} %get-tuple-element.19.cos_ref.cos_hbm, ...), custom_call_target="tpu_custom_call" | custom-call | flops 2147483648 | bytes 8388608 | tf_op jit(solution)/shard_map/sel_project/pallas_call | solution.py:437
  19.9 0.0 copy-done
  19.9 0.8 copy-done.4
  20.7 0.8 copy-done.5
  21.6 0.1 copy.27
  21.6 0.1 broadcast_in_dim.44
  21.7 0.1 reshape.49
  21.9 0.7 broadcast_in_dim.45.bias_ref
  22.5 0.8 dynamic-slice_bitcast_fusion.1
  23.4 0.3 copy.28
  23.7 0.0 copy-start.9
  23.7 1.7 %fusion.1.w_hbm = bf16[2048,640]{1,0:T(8,128)(2,1)} fusion(bf16[2048,8]{1,0:T(8,128)(2,1)S(1)} %copy.28, bf16[2048,128]{1,0:T(8,128)(2,1)S(1)} %copy-done.7, bf16[2048,128]{1,0:T(8,128)(2,1)S(1)} %copy-done.8, bf16[2048,256]{1,0:T(8,128)(2,1)S(1)} %copy-done.6), kind=kLoop, calls=%fused_computation.3 | loop fusion | flops 13107200 | bytes 4751360 | tf_op jit(solution)/shard_map/concatenate | solution.py:454
  25.3 1.3 copy.29.ki_hbm
  26.7 2.4 %copy.30.vi_hbm = bf16[2,2048,64]{2,1,0:T(8,128)(2,1)} copy(bf16[2,2048,64]{1,2,0:T(8,128)(2,1)} %param.28) | data formatting | bytes 1048576 | tf_op args[12]
  29.0 110.4 %exchange.1 = bf16[512,1024]{1,0:T(8,128)(2,1)} custom-call(s32[256]{0:T(256)} %reshape.48.idx_ref, f32[2,16,1,640]{3,2,1,0:T(1,128)} %broadcast_in_dim.45.bias_ref, bf16[1,2048]{1,0:T(2,128)(2,1)} %copy-done.3, bf16[2,32,64]{2,1,0:T(8,128)(2,1)} %ke_ref.1, bf16[2,64,64]{2,1,0:T(8,128)(2,1)} %ko_ref.1, bf16[2,32,64]{2,1,0:T(8,128)(2,1)} %ve_ref.1, ...), custom_call_target="tpu_custom_call" | custom-call | flops 40000000000 | bytes 20000000 | tf_op jit(solution)/shard_map/exchange/pallas_call | solution.py:495
  139.5 6.2 %convolution_convert_fusion = bf16[512,2048]{1,0:T(8,128)(2,1)} fusion(bf16[512,1024]{1,0:T(8,128)(2,1)} %exchange.1, bf16[1024,2048]{1,0:T(8,128)(2,1)} %param.30), kind=kOutput, calls=%fused_computation.2 | convolution fusion | flops 2148532224 | bytes 7340032 | tf_op jit(solution)/shard_map/dot_general | solution.py:532
  (16 shorter events, 0.1 us)
Async XLA Ops:
  4.3 4.6 %copy-start.10 = (bf16[2048]{0:T(1024)(128)(2,1)S(1)}, bf16[2048]{0:T(1024)(128)(2,1)}, u32[]{:S(2)}) copy-start(bf16[2048]{0:T(1024)(128)(2,1)} %param.17) | copy-start | bytes 12292
  8.9 11.0 %copy-start = (f32[2048,128]{1,0:T(8,128)}, f32[2048,128]{1,0:T(8,128)S(1)}, u32[]{:S(2)}) copy-start(f32[2048,128]{1,0:T(8,128)S(1)} %get-tuple-element.17.down_ref.down_hbm) | copy-start | bytes 3145732
  8.9 11.0 %copy-start.1 = (f32[2048,128]{1,0:T(8,128)}, f32[2048,128]{1,0:T(8,128)S(1)}, u32[]{:S(2)}) copy-start(f32[2048,128]{1,0:T(8,128)S(1)} %get-tuple-element.18.up_ref.up_hbm) | copy-start | bytes 3145732
  8.9 11.0 %copy-start.2 = (f32[2048,128]{1,0:T(8,128)}, f32[2048,128]{1,0:T(8,128)S(1)}, u32[]{:S(2)}) copy-start(f32[2048,128]{1,0:T(8,128)S(1)} %get-tuple-element.19.cos_ref.cos_hbm) | copy-start | bytes 3145732
  9.0 10.9 %copy-start.3 = (bf16[1,2048]{1,0:T(2,128)(2,1)}, bf16[1,2048]{1,0:T(2,128)(2,1)S(1)}, u32[]{:S(2)}) copy-start(bf16[1,2048]{1,0:T(2,128)(2,1)S(1)} %reshape.50.gain_ref) | copy-start | bytes 12292
  9.0 14.7 %copy-start.6 = (bf16[2048,256]{1,0:T(8,128)(2,1)S(1)}, bf16[2048,256]{1,0:T(8,128)(2,1)}, u32[]{:S(2)}) copy-start(bf16[2048,256]{1,0:T(8,128)(2,1)} %param.18) | copy-start | bytes 3145732
  9.0 14.7 %copy-start.7 = (bf16[2048,128]{1,0:T(8,128)(2,1)S(1)}, bf16[2048,128]{1,0:T(8,128)(2,1)}, u32[]{:S(2)}) copy-start(bf16[2048,128]{1,0:T(8,128)(2,1)} %param.20) | copy-start | bytes 1572868
  9.0 14.7 %copy-start.8 = (bf16[2048,128]{1,0:T(8,128)(2,1)S(1)}, bf16[2048,128]{1,0:T(8,128)(2,1)}, u32[]{:S(2)}) copy-start(bf16[2048,128]{1,0:T(8,128)(2,1)} %param.19) | copy-start | bytes 1572868
  19.9 0.8 copy-start.4
  20.7 0.8 copy-start.5
  23.7 1.7 %copy-start.9 = (bf16[2,2048,64]{1,2,0:T(8,128)(2,1)S(1)}, bf16[2,2048,64]{1,2,0:T(8,128)(2,1)}, u32[]{:S(2)}) copy-start(bf16[2,2048,64]{1,2,0:T(8,128)(2,1)} %param.25) | copy-start | bytes 1572868
where the time goes:
time: 146 us
  Pallas kernels  121 us (83%)
  local copies, waits for them, and re-layouts  10.2 us (7%)
  other arithmetic  7.78 us (5%)
  matrix products  6.17 us (4%)
    pallas_call x1, Pallas kernels, per_device(): pl.pallas_call(functools.partial(exchange_kernel, planes), in_specs=[pl.B...  110 us
    pallas_call x1, Pallas kernels, per_device(): pl.pallas_call(sel_kernel, grid=(steps,), in_specs=[row_spec(width), full...  10.8 us
    dot_general x1, matrix products, per_device(): jnp.dot(gathered, out_weight, preferred_element_type=f32).astype(bf16)  6.17 us
    unnamed x24, local copies, waits for them, and re-layouts  5.41 us
    select_n x1, other arithmetic, per_device(): down = jnp.where(first, 0.0, sine)  3.79 us

commit v1 on v0

v1 whole, which is shorter than its diff:
```python
import functools

import numpy as np

import jax
import jax.numpy as jnp
from jax import lax
from jax.experimental import pallas as pl
from jax.experimental.pallas import tpu as pltpu
from jax.sharding import PartitionSpec as P

HEAD_DIM = 64
CMP_BLOCK = 32
SEL_BLOCK = 64
Q_BLOCK = 128
LANES = 2 * HEAD_DIM
PLANES = 4
TILE = 256
MESH = pl.DeviceIdType.MESH

ROPE_BASE = 10000.0
norm_eps = 1e-06
MASKED = -1e30

f32 = jnp.float32
bf16 = jnp.bfloat16


def low_lanes(shape):
    return lax.broadcasted_iota(jnp.int32, shape, len(shape) - 1) < HEAD_DIM


def nt_dot(a, b):
    return lax.dot_general(a, b, (((1,), (1,)), ((), ())), preferred_element_type=f32)


def swap(x):
    return pltpu.roll(x, HEAD_DIM, 1)


def turn(x, cosine, sine):
    half = HEAD_DIM // 2
    lane = lax.broadcasted_iota(jnp.int32, x.shape, 1)
    first = lax.rem(lane, HEAD_DIM) < half
    partner = jnp.where(first, pltpu.roll(x, LANES - half, 1), pltpu.roll(x, half, 1))
    return x * cosine + partner * sine


def gate_lanes(gate, first, shape):
    return jnp.where(low_lanes(shape), gate[:, first : first + 1], gate[:, first + 1 : first + 2])


def with_ones(keys):
    return jnp.where(low_lanes(keys.shape), jnp.ones_like(keys), keys)


def settle(out, rows):
    low = low_lanes((rows, LANES))
    value = jnp.where(low, swap(out[:rows]), out[rows:])
    total = jnp.where(low, out[:rows], swap(out[rows:]))
    return value, total


def layer_kernel(planes, pieces, *refs):
    (
        pick,
        gain_ref,
        ke_ref,
        ko_ref,
        ve_ref,
        vo_ref,
        tok_hbm,
        query_hbm,
        branch_hbm,
        ki_hbm,
        vi_hbm,
        wo_hbm,
        fine_hbm,
        coarse_hbm,
    ) = refs[:14]
    piece_hbm, refs = refs[14 : 14 + pieces], refs[14 + pieces :]
    out_ref, refs = refs[0], refs[1:]
    (
        own,
        sel,
        stage_x,
        stage_t,
        tok,
        normed,
        w_kv,
        w_q,
        w_gate,
        wo,
        fine,
        coarse,
        ki,
        vi,
        qp,
        qt,
        ck,
        cv,
        gate,
        sums,
        oc,
        mix,
        got,
        acc,
        tok_sem,
        local_sem,
        own_send,
        col_send,
        col_recv,
        x_send,
        t_send,
        sel_recv,
        sum_send,
        sum_recv,
        mix_send,
        mix_recv,
    ) = refs[:36]
    col = refs[36:]

    kv_local = own.shape[0]
    span = own.shape[1]
    owners, ranks = sums.shape[0], got.shape[0]
    rows, width = tok.shape
    across = owners // planes
    last = planes - 1
    q_blocks = rows // Q_BLOCK
    all_blocks = owners * q_blocks
    blocks = rows // CMP_BLOCK
    tiles = rows // TILE
    rank_rows = rows // ranks
    group = rank_rows // Q_BLOCK
    heads = branch_hbm.shape[1]
    heads_local = 2 * kv_local
    kv_width = kv_local * HEAD_DIM
    scale = HEAD_DIM ** (-0.5)
    me, rank = lax.axis_index("kv"), lax.axis_index("tp")
    z, x = me // across, me % across

    barrier = pltpu.get_barrier_semaphore()
    for d in range(1, owners):
        pl.semaphore_signal(barrier, inc=1, device_id={"kv": (me + d) % owners}, device_id_type=MESH)
    for d in range(1, ranks):
        pl.semaphore_signal(barrier, inc=1, device_id={"tp": (rank + d) % ranks}, device_id_type=MESH)

    def rows_at(i):
        return pl.ds(pl.multiple_of(i * TILE, TILE), TILE)

    def tok_copy(i):
        return pltpu.make_async_copy(tok_hbm.at[rows_at(i)], tok.at[rows_at(i)], tok_sem.at[i])

    early = [(fine_hbm, fine), (coarse_hbm, coarse)]
    first = 0
    for ref in piece_hbm:
        early.append((ref, w_kv.at[:, pl.ds(first, ref.shape[1])]))
        first += ref.shape[1]
    late = [(ki_hbm, ki), (vi_hbm, vi), (query_hbm, w_q)]
    late += [(branch_hbm.at[b], w_gate.at[pl.ds(b * heads, heads)]) for b in range(2)]
    final = [(wo_hbm, wo)]
    copies = [
        pltpu.make_async_copy(a, b, local_sem.at[n]) for n, (a, b) in enumerate(early + late + final)
    ]
    tok_copy(0).start()
    for copy in copies[: len(early)]:
        copy.start()
    for i in range(1, tiles):
        tok_copy(i).start()
    for copy in copies[len(early) :]:
        copy.start()

    w_gate[2 * heads :, :] = jnp.zeros((w_gate.shape[0] - 2 * heads, width), bf16)
    moves = [(dz, dx) for dz in range(planes) for dx in range(across) if (dz, dx) != (0, 0)]

    def slot(dz, dx):
        return dz * across + dx - 1

    def present(dz, dx):
        return (x >= dx) if dz == 0 else (z >= dz)

    for dz, dx in moves:

        def clear(dz=dz, dx=dx):
            for k in range(kv_local):
                sel[slot(dz, dx), k] = jnp.zeros(sel.shape[2:], bf16)

        pl.when(jnp.logical_not(present(dz, dx)))(clear)


    def remote(src, dst, send, recv, target):
        return pltpu.make_async_remote_copy(
            src_ref=src,
            dst_ref=dst,
            send_sem=send,
            recv_sem=recv,
            device_id={"kv": target},
            device_id_type=MESH,
        )

    above = lax.rem(me + across, owners)

    def own_copy(k, at):
        return remote(own.at[k, at], col[k].at[at], own_send.at[k], col_recv.at[k, 0], above)

    def col_of(dz, k):
        return col[(dz - 1) * kv_local + k]

    def up_copy(dz, k):
        return remote(
            col_of(dz, k), col_of(dz + 1, k), col_send.at[k, dz], col_recv.at[k, dz], above
        )

    def side_copy(dz, dx, k):
        return remote(
            stage_x.at[dz, dx - 1, k],
            sel.at[slot(dz, dx), k],
            x_send.at[dz, dx - 1, k],
            sel_recv.at[slot(dz, dx), k, 0],
            z * across + (x + dx) % across,
        )

    def top_copy(dz, dx, k, step):
        at = pl.ds((rank + 1 + step) % ranks * group, group)
        return remote(
            stage_t.at[dz - 1, dx, k, at],
            sel.at[slot(dz + 1, dx), k, at],
            t_send.at[dz - 1, dx, k, step],
            sel_recv.at[slot(dz + 1, dx), k, step],
            lax.rem((z + 1) * across + (x + dx) % across, owners),
        )

    def gather(src, dst, source, k, device):
        base = (source * kv_local + k) * all_blocks + device * q_blocks

        def one(j, carry):
            dst[j] = src[jnp.maximum(pick[base + j], 0)]
            return carry

        lax.fori_loop(0, q_blocks, one, 0, unroll=4)

    def relay(dz, k):
        whole = (z >= dz) & ((z < last) | (dz == 1))

        def go():
            remote(col_of(dz, k), col_of(dz, k), own_send.at[k], col_recv.at[k, dz - 1], above).wait_recv()
            source = me - dz * across
            if dz + 1 < last:
                pl.when(z + 1 < last)(lambda: up_copy(dz, k).start())
            if dz + 1 <= last:

                def to_top():
                    for dx in range(across):
                        gather(
                            col_of(dz, k),
                            stage_t.at[dz - 1, dx, k],
                            source,
                            k,
                            (z + 1) * across + (x + dx) % across,
                        )
                    half = (ranks // 2) if dz + 1 == last and kv_local > 1 else ranks
                    sends = [(s, k) for s in range(half)]
                    if half < ranks and k == kv_local - 1:
                        sends += [(s, n) for s in range(half, ranks) for n in range(kv_local)]
                    for s, n in sends:
                        for dx in range(across):
                            top_copy(dz, dx, n, s).start()

                pl.when(z + 1 == last)(to_top)
            for dx in range(1, across):
                there = z * across + (x + dx) % across
                gather(col_of(dz, k), stage_x.at[dz, dx - 1, k], source, k, there)
                side_copy(dz, dx, k).start()
            gather(col_of(dz, k), sel.at[slot(dz, 0), k], source, k, me)

        pl.when(whole)(go)


    def norm_tile(i):
        t = tok[rows_at(i), :].astype(f32)
        inv = lax.rsqrt(jnp.mean(t * t, axis=-1, keepdims=True) + norm_eps)
        normed[rows_at(i), :] = (t * inv * gain_ref[...].astype(f32)).astype(bf16)

    def tables(i):
        row = pl.ds(me * tiles + i, 1)
        cos_c, sin_c = coarse[0, row, :], coarse[1, row, :]
        return fine[0] * cos_c - fine[1] * sin_c, fine[1] * cos_c + fine[0] * sin_c

    def project_kv(i):
        at = rows_at(i)
        y = jnp.dot(normed[at, :], w_kv[...], preferred_element_type=f32)
        cosine, sine = tables(i)
        here = pl.ds(i * (TILE // SEL_BLOCK), TILE // SEL_BLOCK)
        if kv_local == 1:
            pair = y[:, :LANES]
            packed = [jnp.where(low_lanes(pair.shape), turn(pair, cosine, sine), pair)]
        else:
            packed = []
            for k in range(0, kv_local, 2):
                key = turn(y[:, k * HEAD_DIM : k * HEAD_DIM + LANES], cosine, sine)
                value = y[:, kv_width + k * HEAD_DIM : kv_width + k * HEAD_DIM + LANES]
                low = low_lanes(key.shape)
                packed.append(jnp.where(low, key, swap(value)))
                packed.append(jnp.where(low, swap(key), value))
        for k in range(kv_local):
            own[k, here] = packed[k].astype(bf16).reshape(TILE // SEL_BLOCK, SEL_BLOCK, LANES)
        ck[at, :] = y[:, 2 * kv_width : 3 * kv_width].astype(bf16).astype(f32)
        cv[at, :] = y[:, 3 * kv_width : 4 * kv_width].astype(bf16).astype(f32)

    def send_tile(i):
        here = pl.ds(i * (TILE // SEL_BLOCK), TILE // SEL_BLOCK)
        if planes > 1:
            pl.when(z < last)(lambda: own_copy(0, here).start())

    tok_copy(0).wait()
    norm_tile(0)
    for copy in copies[: len(early)]:
        copy.wait()
    pl.semaphore_wait(barrier, owners + ranks - 2)

    def first_pass(i, carry):
        pl.when(i > 0)(lambda: send_tile(i - 1))
        tok_copy(i + 1).wait()
        norm_tile(i + 1)
        project_kv(i)
        return carry

    lax.fori_loop(0, tiles - 1, first_pass, 0)
    if tiles > 1:
        send_tile(tiles - 2)
    project_kv(tiles - 1)

    for copy in copies[len(early) : len(early) + len(late)]:
        copy.wait()
    send_tile(tiles - 1)


    def summarize(x_ref, e_ref, i_ref, o_ref):
        embed = jnp.concatenate([e_ref[k].astype(f32) for k in range(kv_local)], axis=1)
        parts = [
            x_ref[pl.ds(c, blocks, stride=CMP_BLOCK), :] + embed[c : c + 1] for c in range(CMP_BLOCK)
        ]
        result = []
        for k in range(kv_local):
            if kv_local == 1:
                flat = jnp.concatenate([p.astype(bf16) for p in parts], axis=1)
            else:
                g, odd = k // 2 * LANES, k % 2
                low = low_lanes((blocks, LANES))
                cut = []
                for c in range(0, CMP_BLOCK, 2):
                    a, b = parts[c][:, g : g + LANES], parts[c + 1][:, g : g + LANES]
                    both = jnp.where(low, swap(a), b) if odd else jnp.where(low, a, swap(b))
                    cut.append(both.astype(bf16))
                flat = jnp.concatenate(cut, axis=1)
            hidden = jax.nn.gelu(nt_dot(flat, i_ref[k])).astype(bf16)
            result.append(jnp.dot(hidden, o_ref[k], preferred_element_type=f32))
        return result

    sk = summarize(ck, ke_ref, ki, ko_ref)
    sv = summarize(cv, ve_ref, vi, vo_ref)
    for k in range(kv_local):
        sums[me, k] = jnp.concatenate([sk[k], sv[k]], axis=1).astype(bf16)

    def sum_copy(d, source):
        return remote(
            sums.at[source], sums.at[source], sum_send.at[d], sum_recv.at[d], (me + d) % owners
        )

    for dx in range(1, across):
        for k in range(kv_local):
            gather(own.at[k], stage_x.at[0, dx - 1, k], me, k, z * across + (x + dx) % across)
    for d in range(1, owners):
        sum_copy(d, me).start()
    everything = pl.ds(0, span)
    for k in range(1, kv_local):
        if planes > 1:
            pl.when(z < last)(lambda k=k: own_copy(k, everything).start())
    for dx in range(1, across):
        for k in range(kv_local):
            pl.when(x + dx < across)(lambda dx=dx, k=k: side_copy(0, dx, k).start())


    def second_pass(i, carry):
        at = rows_at(i)
        n = normed[at, :]
        y = jnp.dot(n, w_q[...], preferred_element_type=f32)
        cosine, sine = tables(i)
        for k in range(kv_local):
            v = y[:, k * LANES : (k + 1) * LANES] * scale
            low = low_lanes(v.shape)
            for ref, q in ((qp, v), (qt, turn(v, cosine, sine))):
                ref[k, 0, at, :] = jnp.where(low, q, 0.0).astype(bf16)
                ref[k, 1, at, :] = jnp.where(low, swap(q), 0.0).astype(bf16)
        g = jax.nn.sigmoid(nt_dot(n, w_gate[...]))
        gate[at, :] = pltpu.roll(g, lax.rem(LANES - rank * heads_local, LANES), 1)
        return carry

    lax.fori_loop(0, tiles, second_pass, 0)
    relays = [(dz, k) for dz in range(1, max(2, last)) for k in range(kv_local)] if planes > 1 else []
    if relays:
        relay(*relays[0])


    for d in range(1, owners):
        sum_copy(d, (me + owners - d) % owners).wait_recv()

    def compress(i, carry):
        at = rows_at(i)
        row = lax.broadcasted_iota(jnp.int32, (2 * TILE, 1), 0)
        pos = me * rows + i * TILE + jnp.where(row >= TILE, row - TILE, row)
        lane = lax.broadcasted_iota(jnp.int32, (1, owners * blocks), 1)
        allowed = (lane + 1) * CMP_BLOCK - 1 <= pos
        some = pos[:TILE] >= CMP_BLOCK - 1
        for k in range(kv_local):
            keys = jnp.concatenate([sums[s, k] for s in range(owners)], axis=0)
            q = jnp.concatenate([qp[k, 0, at, :], qp[k, 1, at, :]], axis=0)
            s = jnp.where(allowed, nt_dot(q, keys), MASKED)
            top = jnp.max(s, axis=-1, keepdims=True)
            e = jnp.exp(s - top).astype(bf16)
            o = jnp.dot(e, with_ones(keys), preferred_element_type=f32)
            value, total = settle(o, TILE)
            o = jnp.where(some, value / total, 0.0)
            oc[k, at, :] = o * gate_lanes(gate[at, :], 2 * k, o.shape)
        return carry

    bounds = [tiles * n // max(1, len(relays) - 1) for n in range(max(1, len(relays) - 1) + 1)]
    for n in range(len(bounds) - 1):
        lax.fori_loop(bounds[n], bounds[n + 1], compress, 0)
        if n + 1 < len(relays):
            relay(*relays[n + 1])


    def is_top(dz):
        return (z == last) & (dz >= 2)

    def wait_side(dz, dx, k):
        pl.when(present(dz, dx) & jnp.logical_not(is_top(dz)))(lambda: side_copy(dz, dx, k).wait_recv())

    for dz, dx in moves:
        if dx:
            for k in range(kv_local):
                wait_side(dz, dx, k)

    def mix_copy(step):
        target = (rank + 1 + step) % ranks
        at = pl.ds(pl.multiple_of(target * rank_rows, rank_rows), rank_rows)
        return pltpu.make_async_remote_copy(
            src_ref=mix.at[at],
            dst_ref=got.at[rank],
            send_sem=mix_send.at[step],
            recv_sem=mix_recv.at[step],
            device_id={"tp": target},
            device_id_type=MESH,
        )

    def add_rank(step):
        source = (rank + ranks - 1 - step) % ranks
        mix_copy(step).wait_recv()
        weight = pl.ds(pl.multiple_of(source * kv_local * LANES, LANES), kv_local * LANES)

        def part(i, carry):
            at = pl.ds(pl.multiple_of(i * Q_BLOCK, Q_BLOCK), Q_BLOCK)
            more = jnp.dot(got[source, at, :], wo[weight, :], preferred_element_type=f32)
            acc[at, :] = acc[at, :] + more
            return carry

        lax.fori_loop(0, group, part, 0)

    acc[...] = jnp.zeros_like(acc)
    copies[-1].wait()

    def choose(step, carry):
        pl.when(step > 0)(lambda: mix_copy(step - 1).start())
        target = (rank + 1 + step) % ranks
        pl.when(step > 1)(lambda: add_rank(step - 2))
        for dz, dx in moves:
            if dz >= 2:

                def wait_top(dz=dz, dx=dx):
                    for k in range(kv_local):
                        top_copy(dz - 1, dx, k, step).wait_recv()

                pl.when(is_top(dz))(wait_top)

        def block(u, carry):
            j = target * group + u
            at = pl.ds(pl.multiple_of(j * Q_BLOCK, Q_BLOCK), Q_BLOCK)
            here = me * q_blocks + j
            low = low_lanes((1, LANES))
            row = lax.broadcasted_iota(jnp.int32, (2 * Q_BLOCK, Q_BLOCK), 0)
            row = jnp.where(row >= Q_BLOCK, row - Q_BLOCK, row)
            lane = lax.broadcasted_iota(jnp.int32, row.shape, 1)
            for k in range(kv_local):
                parts = [own[k, j * (Q_BLOCK // SEL_BLOCK) + b] for b in range(Q_BLOCK // SEL_BLOCK)]
                mine = pick[(me * kv_local + k) * all_blocks + here]
                parts.append(own[k, jnp.maximum(mine, 0)])
                usable = [(mine >= 0) & (mine < j * (Q_BLOCK // SEL_BLOCK))]
                for dz, dx in moves:
                    parts.append(sel[slot(dz, dx), k, j])
                    source = lax.rem(me - dz * across - x + (x + across - dx) % across + owners, owners)
                    found = pick[(source * kv_local + k) * all_blocks + here] >= 0
                    usable.append(found & present(dz, dx))
                bias = [jnp.where(u, 0.0, MASKED).astype(f32) for u in usable]
                bias = jnp.concatenate(
                    [jnp.where(low, bias[n], bias[n + 1]) for n in range(0, len(bias), 2)], axis=1
                )
                keys = jnp.concatenate(parts, axis=0)
                q = jnp.concatenate([qt[k, 0, at, :], qt[k, 1, at, :]], axis=0)
                s = nt_dot(q, keys)
                near = jnp.where(lane > row, MASKED, s[:, :Q_BLOCK])
                s = jnp.concatenate([near, s[:, Q_BLOCK:] + bias], axis=1)
                top = jnp.max(s, axis=-1, keepdims=True)
                e = jnp.exp(s - top).astype(bf16)
                o = jnp.dot(e, with_ones(keys), preferred_element_type=f32)
                value, total = settle(o, Q_BLOCK)
                o = value / total
                g = gate_lanes(gate[at, :], heads + 2 * k, o.shape)
                mix[at, k * LANES : (k + 1) * LANES] = (oc[k, at, :] + o * g).astype(bf16)
            return carry

        lax.fori_loop(0, group, block, 0)
        return carry

    lax.fori_loop(0, ranks, choose, 0)


    if ranks > 1:
        add_rank(ranks - 2)
    mine = pl.ds(pl.multiple_of(rank * kv_local * LANES, LANES), kv_local * LANES)

    def finish(i, carry):
        at = pl.ds(pl.multiple_of(i * Q_BLOCK, Q_BLOCK), Q_BLOCK)
        from_mix = pl.ds(pl.multiple_of(rank * rank_rows + i * Q_BLOCK, Q_BLOCK), Q_BLOCK)
        more = jnp.dot(mix[from_mix, :], wo[mine, :], preferred_element_type=f32)
        out_ref[at, :] = (acc[at, :] + more).astype(bf16)
        return carry

    lax.fori_loop(0, group, finish, 0)


    for k in range(kv_local):
        if planes > 1:
            pl.when(z < last)(lambda k=k: own_copy(k, everything).wait_send())
        for dx in range(1, across):
            pl.when(x + dx < across)(lambda dx=dx, k=k: side_copy(0, dx, k).wait_send())
    for dz, k in relays:
        whole = (z >= dz) & ((z < last) | (dz == 1))
        if dz + 1 < last:
            pl.when(whole & (z + 1 < last))(lambda dz=dz, k=k: up_copy(dz, k).wait_send())
        if dz + 1 <= last:

            def sent_top(dz=dz, k=k):
                for s in range(ranks):
                    for dx in range(across):
                        top_copy(dz, dx, k, s).wait_send()

            pl.when(whole & (z + 1 == last))(sent_top)

        def sent_side(dz=dz, k=k):
            for dx in range(1, across):
                side_copy(dz, dx, k).wait_send()

        pl.when(whole)(sent_side)
    for d in range(1, owners):
        sum_copy(d, me).wait_send()
    for step in range(ranks - 1):
        mix_copy(step).wait_send()


def position_tables(rows, owners):
    half = HEAD_DIM // 2
    lane = np.arange(LANES)
    inverse = ROPE_BASE ** (-(lane % half).astype(np.float64) / half)
    sign = np.where(lane % HEAD_DIM < half, -1.0, 1.0)

    def both(positions):
        phase = positions[:, None].astype(np.float64) * inverse[None, :]
        return np.stack([np.cos(phase), np.sin(phase) * sign]).astype(np.float32)

    return both(np.arange(TILE)), both(np.arange(0, owners * rows, TILE))


def per_device(
    tokens,
    norm_gain,
    query_weight,
    cmp_key_weight,
    cmp_value_weight,
    sel_key_weight,
    sel_value_weight,
    branch_weight,
    key_embed,
    key_inner,
    key_outer,
    value_embed,
    value_inner,
    value_outer,
    out_weight,
    chosen,
):
    rows, width = tokens.shape
    kv_local = key_embed.shape[0]
    owners, ranks = lax.axis_size("kv"), lax.axis_size("tp")
    planes = PLANES if owners % PLANES == 0 else 1
    across = owners // planes
    span = rows // SEL_BLOCK
    q_blocks = rows // Q_BLOCK
    blocks = rows // CMP_BLOCK
    rank_rows = rows // ranks
    kv_width = kv_local * HEAD_DIM

    chosen = chosen.transpose(0, 2, 1)
    source = jnp.arange(owners, dtype=jnp.int32)[:, None, None, None]
    hit = chosen[None] // span == source
    picks = jnp.max(jnp.where(hit, chosen[None] % span, -1), axis=2).reshape(-1)

    weights = [sel_key_weight, sel_value_weight, cmp_key_weight, cmp_value_weight]
    if kv_width % LANES:
        weights = [jnp.concatenate(weights, axis=1)]
    fine, coarse = position_tables(rows, owners)
    operands = (
        picks,
        norm_gain.reshape(1, width),
        key_embed,
        key_outer,
        value_embed,
        value_outer,
        tokens,
        query_weight,
        branch_weight.transpose(0, 2, 1),
        key_inner.transpose(0, 2, 1),
        value_inner.transpose(0, 2, 1),
        out_weight,
        jnp.asarray(fine),
        jnp.asarray(coarse),
        *weights,
    )
    vmem = pl.BlockSpec(memory_space=pltpu.VMEM)
    hbm = pl.BlockSpec(memory_space=pl.ANY)
    dma = pltpu.SemaphoreType.DMA
    picked = (q_blocks, SEL_BLOCK, LANES)
    whole = (span, SEL_BLOCK, LANES)
    n_local = 2 + len(weights) + 5 + 1
    down = max(planes - 2, 1)
    return pl.pallas_call(
        functools.partial(layer_kernel, planes, len(weights)),
        in_specs=[pl.BlockSpec(memory_space=pltpu.SMEM)] + [vmem] * 5 + [hbm] * (8 + len(weights)),
        out_specs=vmem,
        out_shape=jax.ShapeDtypeStruct((rank_rows, out_weight.shape[1]), bf16),
        scratch_shapes=[
            pltpu.VMEM((kv_local, *whole), bf16),
            pltpu.VMEM((max(owners - 1, 1), kv_local, *picked), bf16),
            pltpu.VMEM((max(planes - 1, 1), max(across - 1, 1), kv_local, *picked), bf16),
            pltpu.VMEM((down, across, kv_local, *picked), bf16),
            pltpu.VMEM(tokens.shape, bf16),
            pltpu.VMEM(tokens.shape, bf16),
            pltpu.VMEM((width, 4 * kv_width), bf16),
            pltpu.VMEM(query_weight.shape, bf16),
            pltpu.VMEM((LANES, width), bf16),
            pltpu.VMEM(out_weight.shape, bf16),
            pltpu.VMEM(fine.shape, f32),
            pltpu.VMEM(coarse.shape, f32),
            pltpu.VMEM((kv_local, HEAD_DIM, key_inner.shape[1]), bf16),
            pltpu.VMEM((kv_local, HEAD_DIM, key_inner.shape[1]), bf16),
            pltpu.VMEM((kv_local, 2, rows, LANES), bf16),
            pltpu.VMEM((kv_local, 2, rows, LANES), bf16),
            pltpu.VMEM((rows, kv_width), f32),
            pltpu.VMEM((rows, kv_width), f32),
            pltpu.VMEM((rows, LANES), f32),
            pltpu.VMEM((owners, kv_local, blocks, LANES), bf16),
            pltpu.VMEM((kv_local, rows, LANES), f32),
            pltpu.VMEM((rows, kv_local * LANES), bf16),
            pltpu.VMEM((ranks, rank_rows, kv_local * LANES), bf16),
            pltpu.VMEM((rank_rows, out_weight.shape[1]), f32),
            dma((rows // TILE,)),
            dma((n_local,)),
            dma((kv_local,)),
            dma((kv_local, planes)),
            dma((kv_local, planes)),
            dma((max(planes - 1, 1), max(across - 1, 1), kv_local)),
            dma((down, across, kv_local, ranks)),
            dma((max(owners - 1, 1), kv_local, ranks)),
            dma((owners,)),
            dma((owners,)),
            dma((ranks,)),
            dma((ranks,)),
        ]
        + [pltpu.VMEM(whole, bf16)] * (kv_local * max(planes - 1, 1)),
        compiler_params=pltpu.CompilerParams(
            collective_id=0, has_side_effects=True, vmem_limit_bytes=62 * 1024 * 1024
        ),
        cost_estimate=pl.CostEstimate(flops=int(3e10), bytes_accessed=int(2e7), transcendentals=0),
        name="layer",
    )(*operands)


def solution(mesh):
    placed = (
        P("kv", None),
        P(),
        P(None, "tp"),
        P(None, "tp"),
        P(None, "tp"),
        P(None, "tp"),
        P(None, "tp"),
        P(),
        P("tp", None, None),
        P("tp", None, None),
        P("tp", None, None),
        P("tp", None, None),
        P("tp", None, None),
        P("tp", None, None),
        P(),
        P("tp", None, None),
    )
    return jax.shard_map(
        per_device, mesh=mesh, in_specs=placed, out_specs=P(("kv", "tp"), None), check_vma=False
    )
```

time: 146 us -> 97.3 us (0.67)
  Pallas kernels: 121 us -> 90.2 us
  other arithmetic: 7.78 us -> 1.35 us
  matrix products: 6.17 us -> 0 us
  local copies, waits for them, and re-layouts: 10.2 us -> 4.45 us
    pallas_call x2 -> x1, Pallas kernels: 121 us -> 90.2 us  [per_device(): pl.pallas_call(functools.partial(layer_kernel, planes, len(weights)), in_...]
    dot_general x1 -> x0, matrix products: 6.17 us -> none  [per_device(): jnp.dot(gathered, out_weight, preferred_element_type=f32).astype(bf16)]
    select_n x3 -> x1, other arithmetic: 5.35 us -> 0.71 us  [per_device(): hit = chosen[None] // span == source]
    concatenate x3 -> x0, other arithmetic: 2.4 us -> none  [the longest x1 1.65 us: per_device(): jnp.concatenate([query_weight, cmp_key_weight, cmp_value_weight, jnp.pad(...]
    unnamed x24 -> x1, local copies, waits for them, and re-layouts: 5.41 us -> 3.16 us
    slice x1 -> x0, local copies, waits for them, and re-layouts: 1.99 us -> none  [heads_of(): return w[:, k * HEAD_DIM:(k + 1) * HEAD_DIM]]
where the time goes in v1:
time: 97.3 us; the launch traced here: 96 us
  Pallas kernels  90.2 us (93%)
  local copies, waits for them, and re-layouts  4.45 us (5%)
  other arithmetic  1.35 us (1%)
    pallas_call x1, Pallas kernels, per_device(): pl.pallas_call(functools.partial(layer_kernel, planes, len(weights)), in_...  90.2 us
    unnamed x1, local copies, waits for them, and re-layouts  3.16 us

profile of v1, /device:TPU:27, one launch (start us, length us, event | category | flops | bytes accessed | tf_op | source)
XLA Modules:
  0.0 96.0 jit_solution(3717554618426941330)
XLA Ops:
  0.0 1.3 %reshape.33.refs_1_ = bf16[1,2048]{1,0:T(2,128)(2,1)} reshape(bf16[2048]{0:T(1024)(128)(2,1)} %param.19) | data formatting | bytes 8192 | tf_op jit(solution)/shard_map/reshape | solution.py:624
  1.3 0.7 add_select_fusion.1
  2.0 0.6 select_reduce_fusion
  2.6 90.2 %layer.1 = bf16[512,2048]{1,0:T(8,128)(2,1)} custom-call(s32[2048]{0:T(1024)} %bitcast.30, bf16[1,2048]{1,0:T(2,128)(2,1)} %reshape.33.refs_1_, bf16[2,32,64]{2,1,0:T(8,128)(2,1)} %refs_2_.1, bf16[2,64,64]{2,1,0:T(8,128)(2,1)} %refs_3_.1, bf16[2,32,64]{2,1,0:T(8,128)(2,1)} %refs_4_.1, bf16[2,64,64]{2,1,0:T(8,128)(2,1)} %refs_5_.1, ...), custom_call_target="tpu_custom_call" | custom-call | flops 30000001024 | bytes 20000000 | tf_op jit(solution)/shard_map/layer/pallas_call | solution.py:646
  92.8 3.2 %copy.20 = bf16[512,2048]{1,0:T(8,128)(2,1)} copy(bf16[512,2048]{1,0:T(8,128)(2,1)} %layer.1) | data formatting | bytes 4194304

commit v2 on v1

--- a/solution.py
+++ b/solution.py
@@ -16,6 +16,7 @@
 LANES = 2 * HEAD_DIM
 PLANES = 4
 TILE = 256
+ONES = 16
 MESH = pl.DeviceIdType.MESH
 
 ROPE_BASE = 10000.0
@@ -46,29 +47,30 @@
     return x * cosine + partner * sine
 
 
-def gate_lanes(gate, first, shape):
-    return jnp.where(low_lanes(shape), gate[:, first : first + 1], gate[:, first + 1 : first + 2])
-
-
-def with_ones(keys):
-    return jnp.where(low_lanes(keys.shape), jnp.ones_like(keys), keys)
-
-
-def settle(out, rows):
+def pack_pair(keys, turned):
+    rows = turned.shape[0]
     low = low_lanes((rows, LANES))
-    value = jnp.where(low, swap(out[:rows]), out[rows:])
-    total = jnp.where(low, out[:rows], swap(out[rows:]))
-    return value, total
+    return (
+        jnp.where(low, keys[:rows], swap(turned)).astype(bf16),
+        jnp.where(low, keys[rows:], turned).astype(bf16),
+    )
+
+
+def values_of(parts):
+    low = low_lanes(parts[0].shape)
+    pairs = [jnp.where(low, swap(parts[n]), parts[n + 1]) for n in range(0, len(parts), 2)]
+    values = jnp.concatenate(pairs, axis=1)
+    return jnp.concatenate([values, jnp.ones((ONES, values.shape[1]), values.dtype)], axis=0)
 
 
 def layer_kernel(planes, pieces, *refs):
     (
-        pick,
-        gain_ref,
-        ke_ref,
-        ko_ref,
-        ve_ref,
-        vo_ref,
+        chosen_hbm,
+        gain_hbm,
+        ke_hbm,
+        ko_hbm,
+        ve_hbm,
+        vo_hbm,
         tok_hbm,
         query_hbm,
         branch_hbm,
@@ -81,8 +83,19 @@
     piece_hbm, refs = refs[14 : 14 + pieces], refs[14 + pieces :]
     out_ref, refs = refs[0], refs[1:]
     (
+        pick,
+        found,
+        chosen_ref,
+        gain_ref,
+        gain_row,
+        ke_ref,
+        ko_ref,
+        ve_ref,
+        vo_ref,
         own,
         sel,
+        part_out,
+        part_top,
         stage_x,
         stage_t,
         tok,
@@ -90,6 +103,7 @@
         w_kv,
         w_q,
         w_gate,
+        w_own,
         wo,
         fine,
         coarse,
@@ -97,6 +111,7 @@
         vi,
         qp,
         qt,
+        vsum,
         ck,
         cv,
         gate,
@@ -117,19 +132,20 @@
         sum_recv,
         mix_send,
         mix_recv,
-    ) = refs[:36]
-    col = refs[36:]
+    ) = refs[:49]
+    col = refs[49:]
 
     kv_local = own.shape[0]
     span = own.shape[1]
     owners, ranks = sums.shape[0], got.shape[0]
-    rows, width = tok.shape
+    rows, width = normed.shape
     across = owners // planes
     last = planes - 1
     q_blocks = rows // Q_BLOCK
     all_blocks = owners * q_blocks
     blocks = rows // CMP_BLOCK
     tiles = rows // TILE
+    ring = tok.shape[0]
     rank_rows = rows // ranks
     group = rank_rows // Q_BLOCK
     heads = branch_hbm.shape[1]
@@ -149,28 +165,29 @@
         return pl.ds(pl.multiple_of(i * TILE, TILE), TILE)
 
     def tok_copy(i):
-        return pltpu.make_async_copy(tok_hbm.at[rows_at(i)], tok.at[rows_at(i)], tok_sem.at[i])
-
-    early = [(fine_hbm, fine), (coarse_hbm, coarse)]
+        return pltpu.make_async_copy(tok_hbm.at[rows_at(i)], tok.at[lax.rem(i, ring)], tok_sem.at[i])
+
+    early = [(gain_hbm, gain_ref), (fine_hbm, fine), (coarse_hbm, coarse)]
     first = 0
     for ref in piece_hbm:
         early.append((ref, w_kv.at[:, pl.ds(first, ref.shape[1])]))
         first += ref.shape[1]
-    late = [(ki_hbm, ki), (vi_hbm, vi), (query_hbm, w_q)]
+    late = [(chosen_hbm, chosen_ref), (ki_hbm, ki), (vi_hbm, vi), (query_hbm, w_q)]
+    late += [(ke_hbm, ke_ref), (ko_hbm, ko_ref), (ve_hbm, ve_ref), (vo_hbm, vo_ref)]
     late += [(branch_hbm.at[b], w_gate.at[pl.ds(b * heads, heads)]) for b in range(2)]
-    final = [(wo_hbm, wo)]
+    final = [(wo_hbm, wo), (found, pick)]
     copies = [
         pltpu.make_async_copy(a, b, local_sem.at[n]) for n, (a, b) in enumerate(early + late + final)
     ]
+    to_smem = copies.pop()
     tok_copy(0).start()
     for copy in copies[: len(early)]:
         copy.start()
-    for i in range(1, tiles):
+    for i in range(1, min(ring, tiles)):
         tok_copy(i).start()
     for copy in copies[len(early) :]:
         copy.start()
 
-    w_gate[2 * heads :, :] = jnp.zeros((w_gate.shape[0] - 2 * heads, width), bf16)
     moves = [(dz, dx) for dz in range(planes) for dx in range(across) if (dz, dx) != (0, 0)]
 
     def slot(dz, dx):
@@ -186,6 +203,13 @@
                 sel[slot(dz, dx), k] = jnp.zeros(sel.shape[2:], bf16)
 
         pl.when(jnp.logical_not(present(dz, dx)))(clear)
+    for d in range(1, owners):
+
+        def clear_sums(d=d):
+            for k in range(kv_local):
+                sums[me + d, k] = jnp.zeros(sums.shape[2:], bf16)
+
+        pl.when(me + d < owners)(clear_sums)
 
 
     def remote(src, dst, send, recv, target):
@@ -231,10 +255,10 @@
         )
 
     def gather(src, dst, source, k, device):
-        base = (source * kv_local + k) * all_blocks + device * q_blocks
+        row, base = source * kv_local + k, device * q_blocks
 
         def one(j, carry):
-            dst[j] = src[jnp.maximum(pick[base + j], 0)]
+            dst[j] = src[jnp.maximum(pick[row, base + j], 0)]
             return carry
 
         lax.fori_loop(0, q_blocks, one, 0, unroll=4)
@@ -277,9 +301,10 @@
 
 
     def norm_tile(i):
-        t = tok[rows_at(i), :].astype(f32)
+        t = tok[lax.rem(i, ring)].astype(f32)
         inv = lax.rsqrt(jnp.mean(t * t, axis=-1, keepdims=True) + norm_eps)
-        normed[rows_at(i), :] = (t * inv * gain_ref[...].astype(f32)).astype(bf16)
+        normed[rows_at(i), :] = (t * inv * gain_row[...]).astype(bf16)
+        pl.when(i + ring < tiles)(lambda: tok_copy(i + ring).start())
 
     def tables(i):
         row = pl.ds(me * tiles + i, 1)
@@ -290,20 +315,23 @@
         at = rows_at(i)
         y = jnp.dot(normed[at, :], w_kv[...], preferred_element_type=f32)
         cosine, sine = tables(i)
-        here = pl.ds(i * (TILE // SEL_BLOCK), TILE // SEL_BLOCK)
-        if kv_local == 1:
-            pair = y[:, :LANES]
-            packed = [jnp.where(low_lanes(pair.shape), turn(pair, cosine, sine), pair)]
-        else:
-            packed = []
-            for k in range(0, kv_local, 2):
+        for k in range(kv_local):
+            if kv_local == 1:
+                value = y[:, :LANES]
+                key = turn(value, cosine, sine)
+                keys, first = key, HEAD_DIM
+            elif k % 2 == 0:
                 key = turn(y[:, k * HEAD_DIM : k * HEAD_DIM + LANES], cosine, sine)
                 value = y[:, kv_width + k * HEAD_DIM : kv_width + k * HEAD_DIM + LANES]
-                low = low_lanes(key.shape)
-                packed.append(jnp.where(low, key, swap(value)))
-                packed.append(jnp.where(low, swap(key), value))
-        for k in range(kv_local):
-            own[k, here] = packed[k].astype(bf16).reshape(TILE // SEL_BLOCK, SEL_BLOCK, LANES)
+                keys, first = key, 0
+            else:
+                keys, first = swap(key), HEAD_DIM
+            for t in range(TILE // (2 * SEL_BLOCK)):
+                two = slice(t * 2 * SEL_BLOCK, (t + 1) * 2 * SEL_BLOCK)
+                turned = value[two].T[first : first + HEAD_DIM]
+                a, b = pack_pair(keys[two], turned)
+                own[k, i * (TILE // SEL_BLOCK) + 2 * t] = a
+                own[k, i * (TILE // SEL_BLOCK) + 2 * t + 1] = b
         ck[at, :] = y[:, 2 * kv_width : 3 * kv_width].astype(bf16).astype(f32)
         cv[at, :] = y[:, 3 * kv_width : 4 * kv_width].astype(bf16).astype(f32)
 
@@ -312,9 +340,12 @@
         if planes > 1:
             pl.when(z < last)(lambda: own_copy(0, here).start())
 
+    copies[0].wait()
+    for c in range(gain_ref.shape[0]):
+        gain_row[:, c * LANES : (c + 1) * LANES] = gain_ref[c : c + 1, :].astype(f32)
     tok_copy(0).wait()
     norm_tile(0)
-    for copy in copies[: len(early)]:
+    for copy in copies[1 : len(early)]:
         copy.wait()
     pl.semaphore_wait(barrier, owners + ranks - 2)
 
@@ -333,6 +364,14 @@
     for copy in copies[len(early) : len(early) + len(late)]:
         copy.wait()
     send_tile(tiles - 1)
+
+
+    for s in range(owners):
+        for k in range(kv_local):
+            place = chosen_ref[k] - s * span
+            place = jnp.where((place >= 0) & (place < span), place, -1)
+            found[s * kv_local + k : s * kv_local + k + 1, :] = jnp.max(place, axis=0, keepdims=True)
+    to_smem.start()
 
 
     def summarize(x_ref, e_ref, i_ref, o_ref):
@@ -360,26 +399,39 @@
     sk = summarize(ck, ke_ref, ki, ko_ref)
     sv = summarize(cv, ve_ref, vi, vo_ref)
     for k in range(kv_local):
-        sums[me, k] = jnp.concatenate([sk[k], sv[k]], axis=1).astype(bf16)
-
-    def sum_copy(d, source):
-        return remote(
-            sums.at[source], sums.at[source], sum_send.at[d], sum_recv.at[d], (me + d) % owners
-        )
-
+        sums[me, k] = jnp.concatenate([sk[k], sv[k].T], axis=1).astype(bf16)
+
+    def sum_up(dz, source):
+        there = lax.rem(me + dz * across, owners)
+        return remote(sums.at[source], sums.at[source], sum_send.at[0, dz], sum_recv.at[0, dz], there)
+
+    def sum_side(dz, dx, source):
+        there = z * across + (x + dx) % across
+        return remote(sums.at[source], sums.at[source], sum_send.at[dx, dz], sum_recv.at[dx, dz], there)
+
+    for dz in range(1, planes):
+        pl.when(z + dz <= last)(lambda dz=dz: sum_up(dz, me).start())
+    for dx in range(1, across):
+        pl.when(x + dx < across)(lambda dx=dx: sum_side(0, dx, me).start())
+    to_smem.wait()
     for dx in range(1, across):
         for k in range(kv_local):
             gather(own.at[k], stage_x.at[0, dx - 1, k], me, k, z * across + (x + dx) % across)
-    for d in range(1, owners):
-        sum_copy(d, me).start()
     everything = pl.ds(0, span)
     for k in range(1, kv_local):
         if planes > 1:
             pl.when(z < last)(lambda k=k: own_copy(k, everything).start())
     for dx in range(1, across):
-        for k in range(kv_local):
-            pl.when(x + dx < across)(lambda dx=dx, k=k: side_copy(0, dx, k).start())
-
+        pl.when(x + dx < across)(lambda dx=dx: side_copy(0, dx, 0).start())
+
+
+    mine = lax.broadcasted_iota(jnp.int32, (w_own.shape[0], w_gate.shape[0]), 0)
+    branch = jnp.where(mine >= heads_local, 1, 0)
+    wanted = branch * heads + rank * heads_local + mine - branch * heads_local
+    wanted = jnp.where(mine < 2 * heads_local, wanted, -1)
+    source = lax.broadcasted_iota(jnp.int32, mine.shape, 1)
+    chooser = jnp.where(source == wanted, 1.0, 0.0).astype(bf16)
+    w_own[...] = jnp.dot(chooser, w_gate[...], preferred_element_type=f32).astype(bf16)
 
     def second_pass(i, carry):
         at = rows_at(i)
@@ -392,43 +444,65 @@
             for ref, q in ((qp, v), (qt, turn(v, cosine, sine))):
                 ref[k, 0, at, :] = jnp.where(low, q, 0.0).astype(bf16)
                 ref[k, 1, at, :] = jnp.where(low, swap(q), 0.0).astype(bf16)
-        g = jax.nn.sigmoid(nt_dot(n, w_gate[...]))
-        gate[at, :] = pltpu.roll(g, lax.rem(LANES - rank * heads_local, LANES), 1)
+        gate[:, at] = jax.nn.sigmoid(nt_dot(w_own[...], n))
         return carry
 
-    lax.fori_loop(0, tiles, second_pass, 0)
+    lax.fori_loop(0, tiles // 2, second_pass, 0)
+    for dz in range(1, planes):
+
+        def pass_on(dz=dz):
+            below = me - dz * across
+            sum_up(dz, below).wait_recv()
+            for dx in range(1, across):
+                sum_side(dz, dx, below).start()
+
+        pl.when(z >= dz)(pass_on)
+    lax.fori_loop(tiles // 2, tiles, second_pass, 0)
     relays = [(dz, k) for dz in range(1, max(2, last)) for k in range(kv_local)] if planes > 1 else []
+
+
     if relays:
         relay(*relays[0])
-
-
-    for d in range(1, owners):
-        sum_copy(d, (me + owners - d) % owners).wait_recv()
+    for dx in range(1, across):
+        for k in range(1, kv_local):
+            pl.when(x + dx < across)(lambda dx=dx, k=k: side_copy(0, dx, k).start())
+    for dz in range(planes):
+        for dx in range(1, across):
+            there = lax.rem((z - dz + planes) * across + (x + across - dx) % across, owners)
+            pl.when(present(dz, dx))(
+                lambda dz=dz, dx=dx, there=there: sum_side(dz, dx, there).wait_recv()
+            )
+
+    def gate_row(branch, head, at):
+        return gate[branch * heads_local + head : branch * heads_local + head + 1, at]
+
+    for k in range(kv_local):
+        vsum[k] = values_of([sums[s, k] for s in range(owners)])
 
     def compress(i, carry):
         at = rows_at(i)
-        row = lax.broadcasted_iota(jnp.int32, (2 * TILE, 1), 0)
-        pos = me * rows + i * TILE + jnp.where(row >= TILE, row - TILE, row)
-        lane = lax.broadcasted_iota(jnp.int32, (1, owners * blocks), 1)
-        allowed = (lane + 1) * CMP_BLOCK - 1 <= pos
-        some = pos[:TILE] >= CMP_BLOCK - 1
+        lane = lax.broadcasted_iota(jnp.int32, (1, 2 * TILE), 1)
+        pos = me * rows + i * TILE + jnp.where(lane >= TILE, lane - TILE, lane)
+        block = lax.broadcasted_iota(jnp.int32, (owners * blocks, 1), 0)
+        allowed = (block + 1) * CMP_BLOCK - 1 <= pos
         for k in range(kv_local):
             keys = jnp.concatenate([sums[s, k] for s in range(owners)], axis=0)
             q = jnp.concatenate([qp[k, 0, at, :], qp[k, 1, at, :]], axis=0)
-            s = jnp.where(allowed, nt_dot(q, keys), MASKED)
-            top = jnp.max(s, axis=-1, keepdims=True)
+            s = jnp.where(allowed, nt_dot(keys, q), MASKED)
+            top = jnp.max(s, axis=0, keepdims=True)
             e = jnp.exp(s - top).astype(bf16)
-            o = jnp.dot(e, with_ones(keys), preferred_element_type=f32)
-            value, total = settle(o, TILE)
-            o = jnp.where(some, value / total, 0.0)
-            oc[k, at, :] = o * gate_lanes(gate[at, :], 2 * k, o.shape)
+            o = jnp.dot(vsum[k], e, preferred_element_type=f32)
+            o = jnp.where(pos >= CMP_BLOCK - 1, o[:HEAD_DIM] / o[HEAD_DIM : HEAD_DIM + 1], 0.0)
+            for u in range(2):
+                part = o[:, u * TILE : (u + 1) * TILE] * gate_row(0, 2 * k + u, at)
+                oc[k, u * HEAD_DIM : (u + 1) * HEAD_DIM, at] = part
         return carry
 
-    bounds = [tiles * n // max(1, len(relays) - 1) for n in range(max(1, len(relays) - 1) + 1)]
-    for n in range(len(bounds) - 1):
-        lax.fori_loop(bounds[n], bounds[n + 1], compress, 0)
-        if n + 1 < len(relays):
-            relay(*relays[n + 1])
+    bounds = [tiles * n // kv_local for n in range(kv_local + 1)]
+    for k in range(kv_local):
+        if k > 0 and planes > 1:
+            relay(1, k)
+        lax.fori_loop(bounds[k], bounds[k + 1], compress, 0)
 
 
     def is_top(dz):
@@ -437,7 +511,60 @@
     def wait_side(dz, dx, k):
         pl.when(present(dz, dx) & jnp.logical_not(is_top(dz)))(lambda: side_copy(dz, dx, k).wait_recv())
 
-    for dz, dx in moves:
+    def bias_of(usable):
+        return [jnp.where(u, 0.0, MASKED).astype(f32) for u in usable]
+
+    def add_bias(s, bias):
+        cut = [s[n * SEL_BLOCK : (n + 1) * SEL_BLOCK] + b for n, b in enumerate(bias)]
+        return jnp.concatenate(cut, axis=0)
+
+    def far_parts(some_moves, k, j):
+        parts, usable = [], []
+        for dz, dx in some_moves:
+            parts.append(sel[slot(dz, dx), k, j])
+            source = lax.rem(me - dz * across - x + (x + across - dx) % across + owners, owners)
+            usable.append((pick[source * kv_local + k, me * q_blocks + j] >= 0) & present(dz, dx))
+        return parts, usable
+
+    near_moves = [m for m in moves if m[0] < 2]
+    far_moves = [m for m in moves if m[0] >= 2]
+    own_blocks = Q_BLOCK // SEL_BLOCK
+
+    def queries(k, j):
+        at = pl.ds(pl.multiple_of(j * Q_BLOCK, Q_BLOCK), Q_BLOCK)
+        return jnp.concatenate([qt[k, 0, at, :], qt[k, 1, at, :]], axis=0)
+
+    unroll = group if group < 4 else 4
+
+    def near(k, some, carry):
+        row = lax.broadcasted_iota(jnp.int32, (Q_BLOCK, 2 * Q_BLOCK), 0)
+        lane = lax.broadcasted_iota(jnp.int32, row.shape, 1)
+        lane = jnp.where(lane >= Q_BLOCK, lane - Q_BLOCK, lane)
+        for u in range(unroll):
+            j = some * unroll + u
+            parts = [own[k, j * own_blocks + b] for b in range(own_blocks)]
+            mine = pick[me * kv_local + k, me * q_blocks + j]
+            parts.append(own[k, jnp.maximum(mine, 0)])
+            more, usable = far_parts(near_moves, k, j)
+            bias = bias_of([(mine >= 0) & (mine < j * own_blocks)] + usable)
+            parts = parts + more
+            s = nt_dot(jnp.concatenate(parts, axis=0), queries(k, j))
+            close = jnp.where(row > lane, MASKED, s[:Q_BLOCK])
+            s = jnp.concatenate([close, add_bias(s[Q_BLOCK:], bias)], axis=0)
+            top = jnp.max(s, axis=0, keepdims=True)
+            e = jnp.exp(s - top).astype(bf16)
+            part_out[k, j] = jnp.dot(values_of(parts), e, preferred_element_type=f32)
+            part_top[k, j] = top
+        return carry
+
+    for k in range(kv_local):
+        for dz, dx in near_moves:
+            if dx:
+                wait_side(dz, dx, k)
+        lax.fori_loop(0, q_blocks // unroll, functools.partial(near, k), 0)
+        for dz in range(2, last):
+            relay(dz, k)
+    for dz, dx in far_moves:
         if dx:
             for k in range(kv_local):
                 wait_side(dz, dx, k)
@@ -483,56 +610,43 @@
 
                 pl.when(is_top(dz))(wait_top)
 
-        def block(u, carry):
-            j = target * group + u
-            at = pl.ds(pl.multiple_of(j * Q_BLOCK, Q_BLOCK), Q_BLOCK)
-            here = me * q_blocks + j
-            low = low_lanes((1, LANES))
-            row = lax.broadcasted_iota(jnp.int32, (2 * Q_BLOCK, Q_BLOCK), 0)
-            row = jnp.where(row >= Q_BLOCK, row - Q_BLOCK, row)
-            lane = lax.broadcasted_iota(jnp.int32, row.shape, 1)
-            for k in range(kv_local):
-                parts = [own[k, j * (Q_BLOCK // SEL_BLOCK) + b] for b in range(Q_BLOCK // SEL_BLOCK)]
-                mine = pick[(me * kv_local + k) * all_blocks + here]
-                parts.append(own[k, jnp.maximum(mine, 0)])
-                usable = [(mine >= 0) & (mine < j * (Q_BLOCK // SEL_BLOCK))]
-                for dz, dx in moves:
-                    parts.append(sel[slot(dz, dx), k, j])
-                    source = lax.rem(me - dz * across - x + (x + across - dx) % across + owners, owners)
-                    found = pick[(source * kv_local + k) * all_blocks + here] >= 0
-                    usable.append(found & present(dz, dx))
-                bias = [jnp.where(u, 0.0, MASKED).astype(f32) for u in usable]
-                bias = jnp.concatenate(
-                    [jnp.where(low, bias[n], bias[n + 1]) for n in range(0, len(bias), 2)], axis=1
-                )
-                keys = jnp.concatenate(parts, axis=0)
-                q = jnp.concatenate([qt[k, 0, at, :], qt[k, 1, at, :]], axis=0)
-                s = nt_dot(q, keys)
-                near = jnp.where(lane > row, MASKED, s[:, :Q_BLOCK])
-                s = jnp.concatenate([near, s[:, Q_BLOCK:] + bias], axis=1)
-                top = jnp.max(s, axis=-1, keepdims=True)
-                e = jnp.exp(s - top).astype(bf16)
-                o = jnp.dot(e, with_ones(keys), preferred_element_type=f32)
-                value, total = settle(o, Q_BLOCK)
-                o = value / total
-                g = gate_lanes(gate[at, :], heads + 2 * k, o.shape)
-                mix[at, k * LANES : (k + 1) * LANES] = (oc[k, at, :] + o * g).astype(bf16)
+        def block(some, carry):
+            for u, k in [(u, k) for u in range(unroll) for k in range(kv_local)]:
+                j = target * group + some * unroll + u
+                at = pl.ds(pl.multiple_of(j * Q_BLOCK, Q_BLOCK), Q_BLOCK)
+                out, top = part_out[k, j], part_top[k, j]
+                if far_moves:
+                    parts, usable = far_parts(far_moves, k, j)
+                    s = add_bias(nt_dot(jnp.concatenate(parts, axis=0), queries(k, j)), bias_of(usable))
+                    both = jnp.maximum(top, jnp.max(s, axis=0, keepdims=True))
+                    e = jnp.exp(s - both).astype(bf16)
+                    out = out * jnp.exp(top - both)
+                    out = out + jnp.dot(values_of(parts), e, preferred_element_type=f32)
+                o = out[:HEAD_DIM] / out[HEAD_DIM : HEAD_DIM + 1]
+                o = [o[:, n * Q_BLOCK : (n + 1) * Q_BLOCK] * gate_row(1, 2 * k + n, at) for n in range(2)]
+                turned = oc[k, :, at] + jnp.concatenate(o, axis=0)
+                mix[at, k * LANES : (k + 1) * LANES] = turned.T.astype(bf16)
             return carry
 
-        lax.fori_loop(0, group, block, 0)
+        lax.fori_loop(0, group // unroll, block, 0)
         return carry
 
     lax.fori_loop(0, ranks, choose, 0)
 
 
+    previous = (rank + 1) % ranks
     if ranks > 1:
-        add_rank(ranks - 2)
-    mine = pl.ds(pl.multiple_of(rank * kv_local * LANES, LANES), kv_local * LANES)
+        mix_copy(ranks - 2).wait_recv()
+
+    def weight_of(r):
+        return wo[pl.ds(pl.multiple_of(r * kv_local * LANES, LANES), kv_local * LANES), :]
 
     def finish(i, carry):
         at = pl.ds(pl.multiple_of(i * Q_BLOCK, Q_BLOCK), Q_BLOCK)
         from_mix = pl.ds(pl.multiple_of(rank * rank_rows + i * Q_BLOCK, Q_BLOCK), Q_BLOCK)
-        more = jnp.dot(mix[from_mix, :], wo[mine, :], preferred_element_type=f32)
+        more = jnp.dot(mix[from_mix, :], weight_of(rank), preferred_element_type=f32)
+        if ranks > 1:
+            more += jnp.dot(got[previous, at, :], weight_of(previous), preferred_element_type=f32)
         out_ref[at, :] = (acc[at, :] + more).astype(bf16)
         return carry
 
@@ -562,8 +676,12 @@
                 side_copy(dz, dx, k).wait_send()
 
         pl.when(whole)(sent_side)
-    for d in range(1, owners):
-        sum_copy(d, me).wait_send()
+    for dz in range(1, planes):
+        pl.when(z + dz <= last)(lambda dz=dz: sum_up(dz, me).wait_send())
+    for dx in range(1, across):
+        pl.when(x + dx < across)(lambda dx=dx: sum_side(0, dx, me).wait_send())
+        for dz in range(1, planes):
+            pl.when(z >= dz)(lambda dz=dz, dx=dx: sum_side(dz, dx, me - dz * across).wait_send())
     for step in range(ranks - 1):
         mix_copy(step).wait_send()
 
@@ -610,18 +728,13 @@
     rank_rows = rows // ranks
     kv_width = kv_local * HEAD_DIM
 
-    chosen = chosen.transpose(0, 2, 1)
-    source = jnp.arange(owners, dtype=jnp.int32)[:, None, None, None]
-    hit = chosen[None] // span == source
-    picks = jnp.max(jnp.where(hit, chosen[None] % span, -1), axis=2).reshape(-1)
-
     weights = [sel_key_weight, sel_value_weight, cmp_key_weight, cmp_value_weight]
     if kv_width % LANES:
         weights = [jnp.concatenate(weights, axis=1)]
     fine, coarse = position_tables(rows, owners)
     operands = (
-        picks,
-        norm_gain.reshape(1, width),
+        chosen.transpose(0, 2, 1),
+        norm_gain.reshape(width // LANES, LANES),
         key_embed,
         key_outer,
         value_embed,
@@ -641,23 +754,36 @@
     dma = pltpu.SemaphoreType.DMA
     picked = (q_blocks, SEL_BLOCK, LANES)
     whole = (span, SEL_BLOCK, LANES)
-    n_local = 2 + len(weights) + 5 + 1
+    n_local = 3 + len(weights) + 8 + 2 + 2
+    picks = (owners * kv_local, chosen.shape[1])
     down = max(planes - 2, 1)
     return pl.pallas_call(
         functools.partial(layer_kernel, planes, len(weights)),
-        in_specs=[pl.BlockSpec(memory_space=pltpu.SMEM)] + [vmem] * 5 + [hbm] * (8 + len(weights)),
+        in_specs=[hbm] * len(operands),
         out_specs=vmem,
         out_shape=jax.ShapeDtypeStruct((rank_rows, out_weight.shape[1]), bf16),
         scratch_shapes=[
+            pltpu.SMEM(picks, jnp.int32),
+            pltpu.VMEM(picks, jnp.int32),
+            pltpu.VMEM((kv_local, chosen.shape[2], chosen.shape[1]), jnp.int32),
+            pltpu.VMEM((width // LANES, LANES), bf16),
+            pltpu.VMEM((1, width), f32),
+            pltpu.VMEM(key_embed.shape, bf16),
+            pltpu.VMEM(key_outer.shape, bf16),
+            pltpu.VMEM(value_embed.shape, bf16),
+            pltpu.VMEM(value_outer.shape, bf16),
             pltpu.VMEM((kv_local, *whole), bf16),
             pltpu.VMEM((max(owners - 1, 1), kv_local, *picked), bf16),
+            pltpu.VMEM((kv_local, q_blocks, HEAD_DIM + ONES, 2 * Q_BLOCK), f32),
+            pltpu.VMEM((kv_local, q_blocks, 1, 2 * Q_BLOCK), f32),
             pltpu.VMEM((max(planes - 1, 1), max(across - 1, 1), kv_local, *picked), bf16),
             pltpu.VMEM((down, across, kv_local, *picked), bf16),
-            pltpu.VMEM(tokens.shape, bf16),
+            pltpu.VMEM((min(3, rows // TILE), TILE, width), bf16),
             pltpu.VMEM(tokens.shape, bf16),
             pltpu.VMEM((width, 4 * kv_width), bf16),
             pltpu.VMEM(query_weight.shape, bf16),
-            pltpu.VMEM((LANES, width), bf16),
+            pltpu.VMEM((2 * branch_weight.shape[2], width), bf16),
+            pltpu.VMEM((16, width), bf16),
             pltpu.VMEM(out_weight.shape, bf16),
             pltpu.VMEM(fine.shape, f32),
             pltpu.VMEM(coarse.shape, f32),
@@ -665,11 +791,12 @@
             pltpu.VMEM((kv_local, HEAD_DIM, key_inner.shape[1]), bf16),
             pltpu.VMEM((kv_local, 2, rows, LANES), bf16),
             pltpu.VMEM((kv_local, 2, rows, LANES), bf16),
+            pltpu.VMEM((kv_local, HEAD_DIM + ONES, owners * blocks), bf16),
             pltpu.VMEM((rows, kv_width), f32),
             pltpu.VMEM((rows, kv_width), f32),
-            pltpu.VMEM((rows, LANES), f32),
+            pltpu.VMEM((16, rows), f32),
             pltpu.VMEM((owners, kv_local, blocks, LANES), bf16),
-            pltpu.VMEM((kv_local, rows, LANES), f32),
+            pltpu.VMEM((kv_local, LANES, rows), f32),
             pltpu.VMEM((rows, kv_local * LANES), bf16),
             pltpu.VMEM((ranks, rank_rows, kv_local * LANES), bf16),
             pltpu.VMEM((rank_rows, out_weight.shape[1]), f32),
@@ -681,14 +808,14 @@
             dma((max(planes - 1, 1), max(across - 1, 1), kv_local)),
             dma((down, across, kv_local, ranks)),
             dma((max(owners - 1, 1), kv_local, ranks)),
-            dma((owners,)),
-            dma((owners,)),
+            dma((across, planes)),
+            dma((across, planes)),
             dma((ranks,)),
             dma((ranks,)),
         ]
         + [pltpu.VMEM(whole, bf16)] * (kv_local * max(planes - 1, 1)),
         compiler_params=pltpu.CompilerParams(
-            collective_id=0, has_side_effects=True, vmem_limit_bytes=62 * 1024 * 1024
+            collective_id=0, has_side_effects=True, vmem_limit_bytes=60 * 1024 * 1024
         ),
         cost_estimate=pl.CostEstimate(flops=int(3e10), bytes_accessed=int(2e7), transcendentals=0),
         name="layer",

time: 97.3 us -> 88.9 us (0.914)
  Pallas kernels: 90.2 us -> 84.6 us
  other arithmetic: 1.35 us -> 0 us
  local copies, waits for them, and re-layouts: 4.45 us -> 3.16 us
    pallas_call x1, Pallas kernels: 90.2 us -> 84.6 us  [per_device(): pl.pallas_call(functools.partial(layer_kernel, planes, len(weights)), in_...]
    reshape x1 -> x0, local copies, waits for them, and re-layouts: 1.29 us -> none  [per_device(): norm_gain.reshape(1, width)]
where the time goes in v2:
time: 88.9 us; the launch traced here: 87.7 us
  Pallas kernels  84.6 us (95%)
  local copies, waits for them, and re-layouts  3.16 us (4%)
    pallas_call x1, Pallas kernels, per_device(): pl.pallas_call(functools.partial(layer_kernel, planes, len(weights)), in_...  84.6 us
    unnamed x1, local copies, waits for them, and re-layouts  3.16 us

profile of v2, /device:TPU:27, one launch (start us, length us, event | category | flops | bytes accessed | tf_op | source)
XLA Modules:
  0.0 87.7 jit_solution(17652540105224144252)
XLA Ops:
  0.0 84.6 %layer.1 = bf16[512,2048]{1,0:T(8,128)(2,1)} custom-call(s32[2,8,128]{2,1,0:T(8,128)} %bitcast.8, bf16[16,128]{1,0:T(8,128)(2,1)} %bitcast.9, bf16[2,32,64]{2,1,0:T(8,128)(2,1)} %refs_2_.1, bf16[2,64,64]{2,1,0:T(8,128)(2,1)} %refs_3_.1, bf16[2,32,64]{2,1,0:T(8,128)(2,1)} %refs_4_.1, bf16[2,64,64]{2,1,0:T(8,128)(2,1)} %refs_5_.1, bf16[2048,2048]{1,0:T(8,128)(2,1)} %refs_6_.1, ...), custom_call_target="tpu_custom_call" | custom-call | flops 30000001024 | bytes 20000000 | tf_op jit(solution)/shard_map/layer/pallas_call | solution.py:760
  84.6 3.2 %copy.20 = bf16[512,2048]{1,0:T(8,128)(2,1)} copy(bf16[512,2048]{1,0:T(8,128)(2,1)} %layer.1) | data formatting | bytes 4194304

commit v3 on v2

--- a/solution.py
+++ b/solution.py
@@ -127,13 +127,14 @@
         col_recv,
         x_send,
         t_send,
-        sel_recv,
+        near_recv,
+        far_recv,
         sum_send,
         sum_recv,
         mix_send,
         mix_recv,
-    ) = refs[:49]
-    col = refs[49:]
+    ) = refs[:50]
+    col = refs[50:]
 
     kv_local = own.shape[0]
     span = own.shape[1]
@@ -165,7 +166,7 @@
         return pl.ds(pl.multiple_of(i * TILE, TILE), TILE)
 
     def tok_copy(i):
-        return pltpu.make_async_copy(tok_hbm.at[rows_at(i)], tok.at[lax.rem(i, ring)], tok_sem.at[i])
+        return pltpu.make_async_copy(tok_hbm.at[rows_at(i)], tok.at[lax.rem(i, ring)], tok_sem.at[lax.rem(i, ring)])
 
     early = [(gain_hbm, gain_ref), (fine_hbm, fine), (coarse_hbm, coarse)]
     first = 0
@@ -188,6 +189,8 @@
     for copy in copies[len(early) :]:
         copy.start()
 
+    for ref in (qp, qt):
+        ref[:, :, HEAD_DIM:, :] = jnp.zeros((kv_local, 2, HEAD_DIM, rows), bf16)
     moves = [(dz, dx) for dz in range(planes) for dx in range(across) if (dz, dx) != (0, 0)]
 
     def slot(dz, dx):
@@ -232,25 +235,58 @@
 
     def up_copy(dz, k):
         return remote(
-            col_of(dz, k), col_of(dz + 1, k), col_send.at[k, dz], col_recv.at[k, dz], above
+            col_of(dz, k), col_of(dz + 1, k), col_send.at[k, dz - 1], col_recv.at[k, dz], above
         )
 
     def side_copy(dz, dx, k):
         return remote(
             stage_x.at[dz, dx - 1, k],
             sel.at[slot(dz, dx), k],
-            x_send.at[dz, dx - 1, k],
-            sel_recv.at[slot(dz, dx), k, 0],
+            x_send.at[dz if dz else planes + dx - 1],
+            near_recv.at[slot(dz, dx), k],
             z * across + (x + dx) % across,
         )
 
-    def top_copy(dz, dx, k, step):
-        at = pl.ds((rank + 1 + step) % ranks * group, group)
+    def rank_at(step):
+        if ranks % 2:
+            return (rank + 1 + step) % ranks
+        chip = (rank // 2 + 1 + step // 2) % (ranks // 2)
+        return chip * 2 + (rank + step + 1) % 2
+
+    def rank_from(step):
+        if ranks % 2:
+            return (rank + 2 * ranks - 1 - step) % ranks
+        chip = (rank // 2 + ranks - 1 - step // 2) % (ranks // 2)
+        return chip * 2 + (rank + step + 1) % 2
+
+    parts_last = [1] * (kv_local - 1) + [2 if group % 2 == 0 else 1]
+
+    def pieces_of(k):
+        return range(ranks - 1 + parts_last[k])
+
+    def piece_at(piece, k):
+        if isinstance(piece, int) and piece >= ranks - 1:
+            size = group // parts_last[k]
+            return pl.ds(rank * group + (piece - (ranks - 1)) * size, size)
+        return pl.ds(rank_at(piece) * group, group)
+
+    def far_side_copy(dz, dx, k, piece):
+        at = piece_at(piece, k)
+        return remote(
+            stage_x.at[dz, dx - 1, k, at],
+            sel.at[slot(dz, dx), k, at],
+            x_send.at[dz],
+            far_recv.at[k, piece],
+            z * across + (x + dx) % across,
+        )
+
+    def top_copy(dz, dx, k, piece):
+        at = piece_at(piece, k)
         return remote(
             stage_t.at[dz - 1, dx, k, at],
             sel.at[slot(dz + 1, dx), k, at],
-            t_send.at[dz - 1, dx, k, step],
-            sel_recv.at[slot(dz + 1, dx), k, step],
+            t_send.at[dz - 1],
+            far_recv.at[k, piece],
             lax.rem((z + 1) * across + (x + dx) % across, owners),
         )
 
@@ -282,10 +318,7 @@
                             k,
                             (z + 1) * across + (x + dx) % across,
                         )
-                    half = (ranks // 2) if dz + 1 == last and kv_local > 1 else ranks
-                    sends = [(s, k) for s in range(half)]
-                    if half < ranks and k == kv_local - 1:
-                        sends += [(s, n) for s in range(half, ranks) for n in range(kv_local)]
+                    sends = [(s, k) for s in pieces_of(k)]
                     for s, n in sends:
                         for dx in range(across):
                             top_copy(dz, dx, n, s).start()
@@ -294,7 +327,11 @@
             for dx in range(1, across):
                 there = z * across + (x + dx) % across
                 gather(col_of(dz, k), stage_x.at[dz, dx - 1, k], source, k, there)
-                side_copy(dz, dx, k).start()
+                if dz < 2:
+                    side_copy(dz, dx, k).start()
+                else:
+                    for piece in pieces_of(k):
+                        far_side_copy(dz, dx, k, piece).start()
             gather(col_of(dz, k), sel.at[slot(dz, 0), k], source, k, me)
 
         pl.when(whole)(go)
@@ -373,6 +410,11 @@
             found[s * kv_local + k : s * kv_local + k + 1, :] = jnp.max(place, axis=0, keepdims=True)
     to_smem.start()
 
+    quarter = span // 4
+    for k in range(1, kv_local):
+        if planes > 1:
+            pl.when(z < last)(lambda k=k: own_copy(k, pl.ds(0, quarter)).start())
+
 
     def summarize(x_ref, e_ref, i_ref, o_ref):
         embed = jnp.concatenate([e_ref[k].astype(f32) for k in range(kv_local)], axis=1)
@@ -420,7 +462,7 @@
     everything = pl.ds(0, span)
     for k in range(1, kv_local):
         if planes > 1:
-            pl.when(z < last)(lambda k=k: own_copy(k, everything).start())
+            pl.when(z < last)(lambda k=k: own_copy(k, pl.ds(quarter, span - quarter)).start())
     for dx in range(1, across):
         pl.when(x + dx < across)(lambda dx=dx: side_copy(0, dx, 0).start())
 
@@ -440,10 +482,10 @@
         cosine, sine = tables(i)
         for k in range(kv_local):
             v = y[:, k * LANES : (k + 1) * LANES] * scale
-            low = low_lanes(v.shape)
             for ref, q in ((qp, v), (qt, turn(v, cosine, sine))):
-                ref[k, 0, at, :] = jnp.where(low, q, 0.0).astype(bf16)
-                ref[k, 1, at, :] = jnp.where(low, swap(q), 0.0).astype(bf16)
+                turned = q.T.astype(bf16)
+                for u in range(2):
+                    ref[k, u, :HEAD_DIM, at] = turned[u * HEAD_DIM : (u + 1) * HEAD_DIM]
         gate[:, at] = jax.nn.sigmoid(nt_dot(w_own[...], n))
         return carry
 
@@ -487,8 +529,8 @@
         allowed = (block + 1) * CMP_BLOCK - 1 <= pos
         for k in range(kv_local):
             keys = jnp.concatenate([sums[s, k] for s in range(owners)], axis=0)
-            q = jnp.concatenate([qp[k, 0, at, :], qp[k, 1, at, :]], axis=0)
-            s = jnp.where(allowed, nt_dot(keys, q), MASKED)
+            q = jnp.concatenate([qp[k, 0, :, at], qp[k, 1, :, at]], axis=1)
+            s = jnp.where(allowed, jnp.dot(keys, q, preferred_element_type=f32), MASKED)
             top = jnp.max(s, axis=0, keepdims=True)
             e = jnp.exp(s - top).astype(bf16)
             o = jnp.dot(vsum[k], e, preferred_element_type=f32)
@@ -509,7 +551,7 @@
         return (z == last) & (dz >= 2)
 
     def wait_side(dz, dx, k):
-        pl.when(present(dz, dx) & jnp.logical_not(is_top(dz)))(lambda: side_copy(dz, dx, k).wait_recv())
+        pl.when(present(dz, dx))(lambda: side_copy(dz, dx, k).wait_recv())
 
     def bias_of(usable):
         return [jnp.where(u, 0.0, MASKED).astype(f32) for u in usable]
@@ -532,7 +574,11 @@
 
     def queries(k, j):
         at = pl.ds(pl.multiple_of(j * Q_BLOCK, Q_BLOCK), Q_BLOCK)
-        return jnp.concatenate([qt[k, 0, at, :], qt[k, 1, at, :]], axis=0)
+        return jnp.concatenate([qt[k, 0, :, at], qt[k, 1, :, at]], axis=1)
+
+    def scores(parts, k, j):
+        keys = jnp.concatenate(parts, axis=0)
+        return jnp.dot(keys, queries(k, j), preferred_element_type=f32)
 
     unroll = group if group < 4 else 4
 
@@ -540,19 +586,21 @@
         row = lax.broadcasted_iota(jnp.int32, (Q_BLOCK, 2 * Q_BLOCK), 0)
         lane = lax.broadcasted_iota(jnp.int32, row.shape, 1)
         lane = jnp.where(lane >= Q_BLOCK, lane - Q_BLOCK, lane)
-        for u in range(unroll):
-            j = some * unroll + u
+        js = [some * unroll + u for u in range(unroll)]
+        all_parts, ss = [], []
+        for j in js:
             parts = [own[k, j * own_blocks + b] for b in range(own_blocks)]
             mine = pick[me * kv_local + k, me * q_blocks + j]
             parts.append(own[k, jnp.maximum(mine, 0)])
             more, usable = far_parts(near_moves, k, j)
             bias = bias_of([(mine >= 0) & (mine < j * own_blocks)] + usable)
-            parts = parts + more
-            s = nt_dot(jnp.concatenate(parts, axis=0), queries(k, j))
+            all_parts.append(parts + more)
+            s = scores(all_parts[-1], k, j)
             close = jnp.where(row > lane, MASKED, s[:Q_BLOCK])
-            s = jnp.concatenate([close, add_bias(s[Q_BLOCK:], bias)], axis=0)
-            top = jnp.max(s, axis=0, keepdims=True)
-            e = jnp.exp(s - top).astype(bf16)
+            ss.append(jnp.concatenate([close, add_bias(s[Q_BLOCK:], bias)], axis=0))
+        tops = [jnp.max(s, axis=0, keepdims=True) for s in ss]
+        es = [jnp.exp(s - top).astype(bf16) for s, top in zip(ss, tops)]
+        for j, parts, e, top in zip(js, all_parts, es, tops):
             part_out[k, j] = jnp.dot(values_of(parts), e, preferred_element_type=f32)
             part_top[k, j] = top
         return carry
@@ -564,126 +612,142 @@
         lax.fori_loop(0, q_blocks // unroll, functools.partial(near, k), 0)
         for dz in range(2, last):
             relay(dz, k)
-    for dz, dx in far_moves:
-        if dx:
-            for k in range(kv_local):
-                wait_side(dz, dx, k)
-
-    def mix_copy(step):
-        target = (rank + 1 + step) % ranks
+
+    def wait_far(piece, k):
+        if not far_moves:
+            return
+        at = piece_at(piece, k)
+
+        def wait(first, count):
+            region = sel.at[pl.ds(first, count), k, at]
+            remote(region, region, x_send.at[0], far_recv.at[k, piece], above).wait_recv()
+
+        pl.when(z == last)(lambda: wait(slot(2, 0), (planes - 2) * across))
+        if across > 1:
+            for dz in range(2, last):
+                pl.when(z == dz)(lambda: wait(slot(2, 1), across - 1))
+
+    def mix_copy(k, step):
+        target = rank_at(step)
         at = pl.ds(pl.multiple_of(target * rank_rows, rank_rows), rank_rows)
         return pltpu.make_async_remote_copy(
-            src_ref=mix.at[at],
-            dst_ref=got.at[rank],
-            send_sem=mix_send.at[step],
-            recv_sem=mix_recv.at[step],
+            src_ref=mix.at[k, at],
+            dst_ref=got.at[rank, k],
+            send_sem=mix_send.at[k],
+            recv_sem=mix_recv.at[k],
             device_id={"tp": target},
             device_id_type=MESH,
         )
 
-    def add_rank(step):
-        source = (rank + ranks - 1 - step) % ranks
-        mix_copy(step).wait_recv()
-        weight = pl.ds(pl.multiple_of(source * kv_local * LANES, LANES), kv_local * LANES)
-
-        def part(i, carry):
-            at = pl.ds(pl.multiple_of(i * Q_BLOCK, Q_BLOCK), Q_BLOCK)
-            more = jnp.dot(got[source, at, :], wo[weight, :], preferred_element_type=f32)
-            acc[at, :] = acc[at, :] + more
+    def outputs(k, u):
+        at = pl.ds(pl.multiple_of(u * Q_BLOCK, Q_BLOCK), Q_BLOCK)
+        from_mix = pl.ds(pl.multiple_of(rank * rank_rows + u * Q_BLOCK, Q_BLOCK), Q_BLOCK)
+        shares, weights = [], []
+        for step in range(ranks):
+            source = rank_from(step) if step < ranks - 1 else rank
+            shares.append(got[source, k, at, :] if step < ranks - 1 else mix[k, from_mix, :])
+            weights.append(wo[pl.ds(pl.multiple_of((source * kv_local + k) * LANES, LANES), LANES), :])
+        shares, weights = jnp.concatenate(shares, axis=1), jnp.concatenate(weights, axis=0)
+        return at, jnp.dot(shares, weights, preferred_element_type=f32)
+
+    def every_mix(k):
+        return pltpu.make_async_remote_copy(
+            src_ref=got.at[pl.ds(0, ranks - 1), k],
+            dst_ref=got.at[pl.ds(0, ranks - 1), k],
+            send_sem=mix_send.at[k],
+            recv_sem=mix_recv.at[k],
+            device_id={"tp": rank_at(0)},
+            device_id_type=MESH,
+        )
+
+    def add_head(k):
+        every_mix(k).wait_recv()
+
+        def part(u, carry):
+            at, more = outputs(k, u)
+            acc[at, :] = more if k == 0 else acc[at, :] + more
             return carry
 
         lax.fori_loop(0, group, part, 0)
 
-    acc[...] = jnp.zeros_like(acc)
     copies[-1].wait()
 
-    def choose(step, carry):
-        pl.when(step > 0)(lambda: mix_copy(step - 1).start())
-        target = (rank + 1 + step) % ranks
-        pl.when(step > 1)(lambda: add_rank(step - 2))
-        for dz, dx in moves:
-            if dz >= 2:
-
-                def wait_top(dz=dz, dx=dx):
-                    for k in range(kv_local):
-                        top_copy(dz - 1, dx, k, step).wait_recv()
-
-                pl.when(is_top(dz))(wait_top)
-
-        def block(some, carry):
-            for u, k in [(u, k) for u in range(unroll) for k in range(kv_local)]:
-                j = target * group + some * unroll + u
-                at = pl.ds(pl.multiple_of(j * Q_BLOCK, Q_BLOCK), Q_BLOCK)
-                out, top = part_out[k, j], part_top[k, j]
-                if far_moves:
-                    parts, usable = far_parts(far_moves, k, j)
-                    s = add_bias(nt_dot(jnp.concatenate(parts, axis=0), queries(k, j)), bias_of(usable))
-                    both = jnp.maximum(top, jnp.max(s, axis=0, keepdims=True))
-                    e = jnp.exp(s - both).astype(bf16)
-                    out = out * jnp.exp(top - both)
-                    out = out + jnp.dot(values_of(parts), e, preferred_element_type=f32)
-                o = out[:HEAD_DIM] / out[HEAD_DIM : HEAD_DIM + 1]
-                o = [o[:, n * Q_BLOCK : (n + 1) * Q_BLOCK] * gate_row(1, 2 * k + n, at) for n in range(2)]
-                turned = oc[k, :, at] + jnp.concatenate(o, axis=0)
-                mix[at, k * LANES : (k + 1) * LANES] = turned.T.astype(bf16)
-            return carry
-
-        lax.fori_loop(0, group // unroll, block, 0)
+    def late(k, blocks_of):
+        ats = [pl.ds(pl.multiple_of(j * Q_BLOCK, Q_BLOCK), Q_BLOCK) for j in blocks_of]
+        outs = [part_out[k, j] for j in blocks_of]
+        if far_moves:
+            fars = [far_parts(far_moves, k, j) for j in blocks_of]
+            ss = [scores(parts, k, j) for (parts, _), j in zip(fars, blocks_of)]
+            ss = [add_bias(s, bias_of(usable)) for s, (_, usable) in zip(ss, fars)]
+            old = [part_top[k, j] for j in blocks_of]
+            new = [jnp.maximum(t, jnp.max(s, axis=0, keepdims=True)) for t, s in zip(old, ss)]
+            es = [jnp.exp(s - t).astype(bf16) for s, t in zip(ss, new)]
+            more = [
+                jnp.dot(values_of(parts), e, preferred_element_type=f32) for (parts, _), e in zip(fars, es)
+            ]
+            outs = [o * jnp.exp(a - b) + m for o, a, b, m in zip(outs, old, new, more)]
+        for at, out in zip(ats, outs):
+            o = out[:HEAD_DIM] / out[HEAD_DIM : HEAD_DIM + 1]
+            o = [o[:, n * Q_BLOCK : (n + 1) * Q_BLOCK] * gate_row(1, 2 * k + n, at) for n in range(2)]
+            turned = oc[k, :, at] + jnp.concatenate(o, axis=0)
+            mix[k, at, :] = turned.T.astype(bf16)
+
+    def choose(k, step, carry):
+        pl.when((step > 0) & (step < ranks - 2))(lambda: mix_copy(k, step - 1).start())
+        wait_far(step, k)
+        late(k, [rank_at(step) * group + u for u in range(group)])
         return carry
 
-    lax.fori_loop(0, ranks, choose, 0)
-
-
-    previous = (rank + 1) % ranks
-    if ranks > 1:
-        mix_copy(ranks - 2).wait_recv()
-
-    def weight_of(r):
-        return wo[pl.ds(pl.multiple_of(r * kv_local * LANES, LANES), kv_local * LANES), :]
-
-    def finish(i, carry):
-        at = pl.ds(pl.multiple_of(i * Q_BLOCK, Q_BLOCK), Q_BLOCK)
-        from_mix = pl.ds(pl.multiple_of(rank * rank_rows + i * Q_BLOCK, Q_BLOCK), Q_BLOCK)
-        more = jnp.dot(mix[from_mix, :], weight_of(rank), preferred_element_type=f32)
-        if ranks > 1:
-            more += jnp.dot(got[previous, at, :], weight_of(previous), preferred_element_type=f32)
-        out_ref[at, :] = (acc[at, :] + more).astype(bf16)
-        return carry
-
-    lax.fori_loop(0, group, finish, 0)
+    for k in range(kv_local):
+        lax.fori_loop(0, ranks - 2, functools.partial(choose, k), 0)
+        if ranks > 2:
+            mix_copy(k, ranks - 3).start()
+        if k > 0:
+            add_head(k - 1)
+        lax.fori_loop(ranks - 2, ranks - 1, functools.partial(choose, k), 0)
+        mix_copy(k, ranks - 2).start()
+        size = group // parts_last[k]
+        for n in range(parts_last[k]):
+            wait_far(ranks - 1 + n, k)
+            mine = [n * size + u for u in range(size)]
+            late(k, [rank * group + u for u in mine])
+            if k == kv_local - 1:
+                if n == 0:
+                    every_mix(k).wait_recv()
+                for u in mine:
+                    at, more = outputs(k, u)
+                    out_ref[at, :] = (more if k == 0 else acc[at, :] + more).astype(bf16)
 
 
     for k in range(kv_local):
         if planes > 1:
             pl.when(z < last)(lambda k=k: own_copy(k, everything).wait_send())
-        for dx in range(1, across):
-            pl.when(x + dx < across)(lambda dx=dx, k=k: side_copy(0, dx, k).wait_send())
+
+    def sent(region, send):
+        return remote(region, region, send, sum_recv.at[0, 0], above)
+
+    for dx in range(1, across):
+        pl.when(x + dx < across)(
+            lambda dx=dx: sent(stage_x.at[0, dx - 1], x_send.at[planes + dx - 1]).wait_send()
+        )
     for dz, k in relays:
         whole = (z >= dz) & ((z < last) | (dz == 1))
         if dz + 1 < last:
             pl.when(whole & (z + 1 < last))(lambda dz=dz, k=k: up_copy(dz, k).wait_send())
-        if dz + 1 <= last:
-
-            def sent_top(dz=dz, k=k):
-                for s in range(ranks):
-                    for dx in range(across):
-                        top_copy(dz, dx, k, s).wait_send()
-
-            pl.when(whole & (z + 1 == last))(sent_top)
-
-        def sent_side(dz=dz, k=k):
-            for dx in range(1, across):
-                side_copy(dz, dx, k).wait_send()
-
-        pl.when(whole)(sent_side)
+        if k == 0 and dz + 1 <= last:
+            pl.when(whole & (z + 1 == last))(
+                lambda dz=dz: sent(stage_t.at[dz - 1], t_send.at[dz - 1]).wait_send()
+            )
+        if k == 0 and across > 1:
+            pl.when(whole)(lambda dz=dz: sent(stage_x.at[dz], x_send.at[dz]).wait_send())
     for dz in range(1, planes):
         pl.when(z + dz <= last)(lambda dz=dz: sum_up(dz, me).wait_send())
     for dx in range(1, across):
         pl.when(x + dx < across)(lambda dx=dx: sum_side(0, dx, me).wait_send())
         for dz in range(1, planes):
             pl.when(z >= dz)(lambda dz=dz, dx=dx: sum_side(dz, dx, me - dz * across).wait_send())
-    for step in range(ranks - 1):
-        mix_copy(step).wait_send()
+    for k in range(kv_local):
+        every_mix(k).wait_send()
 
 
 def position_tables(rows, owners):
@@ -757,11 +821,12 @@
     n_local = 3 + len(weights) + 8 + 2 + 2
     picks = (owners * kv_local, chosen.shape[1])
     down = max(planes - 2, 1)
+    n_pieces = ranks + 1
     return pl.pallas_call(
         functools.partial(layer_kernel, planes, len(weights)),
         in_specs=[hbm] * len(operands),
         out_specs=vmem,
-        out_shape=jax.ShapeDtypeStruct((rank_rows, out_weight.shape[1]), bf16),
+        out_shape=pltpu.VMEM((rank_rows, out_weight.shape[1]), bf16),
         scratch_shapes=[
             pltpu.SMEM(picks, jnp.int32),
             pltpu.VMEM(picks, jnp.int32),
@@ -789,33 +854,34 @@
             pltpu.VMEM(coarse.shape, f32),
             pltpu.VMEM((kv_local, HEAD_DIM, key_inner.shape[1]), bf16),
             pltpu.VMEM((kv_local, HEAD_DIM, key_inner.shape[1]), bf16),
-            pltpu.VMEM((kv_local, 2, rows, LANES), bf16),
-            pltpu.VMEM((kv_local, 2, rows, LANES), bf16),
+            pltpu.VMEM((kv_local, 2, LANES, rows), bf16),
+            pltpu.VMEM((kv_local, 2, LANES, rows), bf16),
             pltpu.VMEM((kv_local, HEAD_DIM + ONES, owners * blocks), bf16),
             pltpu.VMEM((rows, kv_width), f32),
             pltpu.VMEM((rows, kv_width), f32),
             pltpu.VMEM((16, rows), f32),
             pltpu.VMEM((owners, kv_local, blocks, LANES), bf16),
             pltpu.VMEM((kv_local, LANES, rows), f32),
-            pltpu.VMEM((rows, kv_local * LANES), bf16),
-            pltpu.VMEM((ranks, rank_rows, kv_local * LANES), bf16),
+            pltpu.VMEM((kv_local, rows, LANES), bf16),
+            pltpu.VMEM((ranks, kv_local, rank_rows, LANES), bf16),
             pltpu.VMEM((rank_rows, out_weight.shape[1]), f32),
-            dma((rows // TILE,)),
+            dma((min(3, rows // TILE),)),
             dma((n_local,)),
             dma((kv_local,)),
-            dma((kv_local, planes)),
-            dma((kv_local, planes)),
-            dma((max(planes - 1, 1), max(across - 1, 1), kv_local)),
-            dma((down, across, kv_local, ranks)),
-            dma((max(owners - 1, 1), kv_local, ranks)),
+            dma((kv_local, down)),
+            dma((kv_local, max(planes - 1, 1))),
+            dma((planes + across,)),
+            dma((down,)),
+            dma((max(2 * across - 1, 1), kv_local)),
+            dma((kv_local, n_pieces)),
             dma((across, planes)),
             dma((across, planes)),
-            dma((ranks,)),
-            dma((ranks,)),
+            dma((kv_local,)),
+            dma((kv_local,)),
         ]
         + [pltpu.VMEM(whole, bf16)] * (kv_local * max(planes - 1, 1)),
         compiler_params=pltpu.CompilerParams(
-            collective_id=0, has_side_effects=True, vmem_limit_bytes=60 * 1024 * 1024
+            collective_id=0, has_side_effects=True, vmem_limit_bytes=56 * 1024 * 1024
         ),
         cost_estimate=pl.CostEstimate(flops=int(3e10), bytes_accessed=int(2e7), transcendentals=0),
         name="layer",

time: 88.9 us -> 81.8 us (0.920)
  Pallas kernels: 84.6 us -> 79.2 us
  local copies, waits for them, and re-layouts: 3.16 us -> 1.32 us
    pallas_call x1, Pallas kernels: 84.6 us -> 79.2 us  [per_device(): pl.pallas_call(functools.partial(layer_kernel, planes, len(weights)), in_...]
    unnamed x1, local copies, waits for them, and re-layouts: 3.16 us -> 1.32 us
where the time goes in v3:
time: 81.8 us; the launch traced here: 80.6 us
  Pallas kernels  79.2 us (97%)
  local copies, waits for them, and re-layouts  1.32 us (2%)
    pallas_call x1, Pallas kernels, per_device(): pl.pallas_call(functools.partial(layer_kernel, planes, len(weights)), in_...  79.2 us

profile of v3, /device:TPU:27, one launch (start us, length us, event | category | flops | bytes accessed | tf_op | source)
XLA Modules:
  0.0 80.6 jit_solution(8968183868280687294)
XLA Ops:
  0.0 79.2 %layer.1 = bf16[512,2048]{1,0:T(8,128)(2,1)S(1)} custom-call(s32[2,8,128]{2,1,0:T(8,128)} %bitcast.8, bf16[16,128]{1,0:T(8,128)(2,1)} %bitcast.9, bf16[2,32,64]{2,1,0:T(8,128)(2,1)} %refs_2_.1, bf16[2,64,64]{2,1,0:T(8,128)(2,1)} %refs_3_.1, bf16[2,32,64]{2,1,0:T(8,128)(2,1)} %refs_4_.1, bf16[2,64,64]{2,1,0:T(8,128)(2,1)} %refs_5_.1, ...), custom_call_target="tpu_custom_call" | custom-call | flops 30000001024 | bytes 20000000 | tf_op jit(solution)/shard_map/layer/pallas_call | solution.py:825
  79.2 1.3 %copy.20 = bf16[512,2048]{1,0:T(8,128)(2,1)} copy(bf16[512,2048]{1,0:T(8,128)(2,1)S(1)} %layer.1) | data formatting | bytes 4194304

commit v4 on v3

--- a/solution.py
+++ b/solution.py
@@ -184,10 +184,8 @@
     tok_copy(0).start()
     for copy in copies[: len(early)]:
         copy.start()
-    for i in range(1, min(ring, tiles)):
-        tok_copy(i).start()
-    for copy in copies[len(early) :]:
-        copy.start()
+    if tiles > 1:
+        tok_copy(1).start()
 
     for ref in (qp, qt):
         ref[:, :, HEAD_DIM:, :] = jnp.zeros((kv_local, 2, HEAD_DIM, rows), bf16)
@@ -384,6 +382,10 @@
     norm_tile(0)
     for copy in copies[1 : len(early)]:
         copy.wait()
+    for i in range(2, min(ring, tiles)):
+        tok_copy(i).start()
+    for copy in copies[len(early) :]:
+        copy.start()
     pl.semaphore_wait(barrier, owners + ranks - 2)
 
     def first_pass(i, carry):
@@ -639,9 +641,9 @@
             device_id_type=MESH,
         )
 
-    def outputs(k, u):
-        at = pl.ds(pl.multiple_of(u * Q_BLOCK, Q_BLOCK), Q_BLOCK)
-        from_mix = pl.ds(pl.multiple_of(rank * rank_rows + u * Q_BLOCK, Q_BLOCK), Q_BLOCK)
+    def outputs(k, u, size):
+        at = pl.ds(pl.multiple_of(u * Q_BLOCK, Q_BLOCK), size * Q_BLOCK)
+        from_mix = pl.ds(pl.multiple_of(rank * rank_rows + u * Q_BLOCK, Q_BLOCK), size * Q_BLOCK)
         shares, weights = [], []
         for step in range(ranks):
             source = rank_from(step) if step < ranks - 1 else rank
@@ -663,12 +665,14 @@
     def add_head(k):
         every_mix(k).wait_recv()
 
-        def part(u, carry):
-            at, more = outputs(k, u)
+        two = 2 if group % 2 == 0 else 1
+
+        def part(n, carry):
+            at, more = outputs(k, n * two, two)
             acc[at, :] = more if k == 0 else acc[at, :] + more
             return carry
 
-        lax.fori_loop(0, group, part, 0)
+        lax.fori_loop(0, group // two, part, 0)
 
     copies[-1].wait()
 
@@ -714,9 +718,8 @@
             if k == kv_local - 1:
                 if n == 0:
                     every_mix(k).wait_recv()
-                for u in mine:
-                    at, more = outputs(k, u)
-                    out_ref[at, :] = (more if k == 0 else acc[at, :] + more).astype(bf16)
+                at, more = outputs(k, n * size, size)
+                out_ref[at, :] = (more if k == 0 else acc[at, :] + more).astype(bf16)
 
 
     for k in range(kv_local):

time: 81.8 us -> 81.3 us (level)
  no operation moved by 1% of the time
where the time goes in v4:
time: 81.3 us; the launch traced here: 80 us
  Pallas kernels  78.7 us (97%)
  local copies, waits for them, and re-layouts  1.32 us (2%)
    pallas_call x1, Pallas kernels, per_device(): pl.pallas_call(functools.partial(layer_kernel, planes, len(weights)), in_...  78.7 us

profile of v4, /device:TPU:27, one launch (start us, length us, event | category | flops | bytes accessed | tf_op | source)
XLA Modules:
  0.0 80.0 jit_solution(16485153821262805056)
XLA Ops:
  0.0 78.7 %layer.1 = bf16[512,2048]{1,0:T(8,128)(2,1)S(1)} custom-call(s32[2,8,128]{2,1,0:T(8,128)} %bitcast.8, bf16[16,128]{1,0:T(8,128)(2,1)} %bitcast.9, bf16[2,32,64]{2,1,0:T(8,128)(2,1)} %refs_2_.1, bf16[2,64,64]{2,1,0:T(8,128)(2,1)} %refs_3_.1, bf16[2,32,64]{2,1,0:T(8,128)(2,1)} %refs_4_.1, bf16[2,64,64]{2,1,0:T(8,128)(2,1)} %refs_5_.1, ...), custom_call_target="tpu_custom_call" | custom-call | flops 30000001024 | bytes 20000000 | tf_op jit(solution)/shard_map/layer/pallas_call | solution.py:828
  78.7 1.3 %copy.20 = bf16[512,2048]{1,0:T(8,128)(2,1)} copy(bf16[512,2048]{1,0:T(8,128)(2,1)S(1)} %layer.1) | data formatting | bytes 4194304

commit v5 on v4

--- a/solution.py
+++ b/solution.py
@@ -98,6 +98,12 @@
         part_top,
         stage_x,
         stage_t,
+        help_q,
+        help_sel,
+        help_out,
+        help_stat,
+        got_out,
+        got_stat,
         tok,
         normed,
         w_kv,
@@ -133,8 +139,13 @@
         sum_recv,
         mix_send,
         mix_recv,
-    ) = refs[:50]
-    col = refs[50:]
+        query_send,
+        query_recv,
+        help_recv,
+        answer_send,
+        answer_recv,
+    ) = refs[:61]
+    col = refs[61:]
 
     kv_local = own.shape[0]
     span = own.shape[1]
@@ -257,19 +268,13 @@
         chip = (rank // 2 + ranks - 1 - step // 2) % (ranks // 2)
         return chip * 2 + (rank + step + 1) % 2
 
-    parts_last = [1] * (kv_local - 1) + [2 if group % 2 == 0 else 1]
-
-    def pieces_of(k):
-        return range(ranks - 1 + parts_last[k])
-
-    def piece_at(piece, k):
-        if isinstance(piece, int) and piece >= ranks - 1:
-            size = group // parts_last[k]
-            return pl.ds(rank * group + (piece - (ranks - 1)) * size, size)
+    own_group = pl.ds(rank * group, group)
+
+    def piece_at(piece):
         return pl.ds(rank_at(piece) * group, group)
 
     def far_side_copy(dz, dx, k, piece):
-        at = piece_at(piece, k)
+        at = piece_at(piece)
         return remote(
             stage_x.at[dz, dx - 1, k, at],
             sel.at[slot(dz, dx), k, at],
@@ -279,14 +284,32 @@
         )
 
     def top_copy(dz, dx, k, piece):
-        at = piece_at(piece, k)
+        at = piece_at(piece)
         return remote(
             stage_t.at[dz - 1, dx, k, at],
             sel.at[slot(dz + 1, dx), k, at],
-            t_send.at[dz - 1],
+            t_send.at[dz - 1, 0 if dx == 0 else 1],
             far_recv.at[k, piece],
             lax.rem((z + 1) * across + (x + dx) % across, owners),
         )
+
+    def help_copy(dz, dx, k):
+        return remote(
+            stage_t.at[dz - 1, dx, k, own_group],
+            help_sel.at[dz - 1, dx - 1, k],
+            t_send.at[dz - 1, 1],
+            help_recv.at[k],
+            z * across + (x + dx) % across,
+        )
+
+    def help_queries():
+        at = pl.ds(pl.multiple_of(rank * rank_rows, rank_rows), rank_rows)
+        below = lax.rem(me + owners - across, owners)
+        return remote(qt.at[:, :, :, at], help_q, query_send.at[0], query_recv.at[0], below)
+
+    def help_answer(k, n):
+        src, dst = ((help_out, got_out), (help_stat, got_stat))[n]
+        return remote(src.at[k], dst.at[k], answer_send.at[k, n], answer_recv.at[k, n], above)
 
     def gather(src, dst, source, k, device):
         row, base = source * kv_local + k, device * q_blocks
@@ -316,10 +339,11 @@
                             k,
                             (z + 1) * across + (x + dx) % across,
                         )
-                    sends = [(s, k) for s in pieces_of(k)]
-                    for s, n in sends:
+                    for dx in range(1, across):
+                        help_copy(dz, dx, k).start()
+                    for s in range(ranks - 1):
                         for dx in range(across):
-                            top_copy(dz, dx, n, s).start()
+                            top_copy(dz, dx, k, s).start()
 
                 pl.when(z + 1 == last)(to_top)
             for dx in range(1, across):
@@ -328,7 +352,7 @@
                 if dz < 2:
                     side_copy(dz, dx, k).start()
                 else:
-                    for piece in pieces_of(k):
+                    for piece in range(ranks):
                         far_side_copy(dz, dx, k, piece).start()
             gather(col_of(dz, k), sel.at[slot(dz, 0), k], source, k, me)
 
@@ -502,6 +526,8 @@
 
         pl.when(z >= dz)(pass_on)
     lax.fori_loop(tiles // 2, tiles, second_pass, 0)
+    if planes > 2:
+        pl.when(z == last)(lambda: help_queries().start())
     relays = [(dz, k) for dz in range(1, max(2, last)) for k in range(kv_local)] if planes > 1 else []
 
 
@@ -583,6 +609,40 @@
         return jnp.dot(keys, queries(k, j), preferred_element_type=f32)
 
     unroll = group if group < 4 else 4
+
+    def answer(k):
+        def go():
+            if k == 0:
+                help_queries().wait_recv()
+            if across > 1:
+                everyone = help_sel.at[:, :, k]
+                remote(everyone, everyone, t_send.at[0, 0], help_recv.at[k], above).wait_recv()
+            fars, ss = [], []
+            for u in range(group):
+                parts, usable = [], []
+                for dz in range(1, planes - 1):
+                    for dx in range(across):
+                        block = stage_t[dz - 1, 0, k, rank * group + u] if dx == 0 else help_sel[dz - 1, dx - 1, k, u]
+                        source = lax.rem((z - dz + planes) * across + (x + across - dx) % across, owners)
+                        there = lax.rem(me + across, owners) * q_blocks + rank * group + u
+                        parts.append(block)
+                        usable.append(pick[source * kv_local + k, there] >= 0)
+                cut = slice(u * Q_BLOCK, (u + 1) * Q_BLOCK)
+                q = jnp.concatenate([help_q[k, 0, :, cut], help_q[k, 1, :, cut]], axis=1)
+                s = jnp.dot(jnp.concatenate(parts, axis=0), q, preferred_element_type=f32)
+                fars.append(parts)
+                ss.append(add_bias(s, bias_of(usable)))
+            tops = [jnp.max(s, axis=0, keepdims=True) for s in ss]
+            es = [jnp.exp(s - t).astype(bf16) for s, t in zip(ss, tops)]
+            outs = [jnp.dot(values_of(p), e, preferred_element_type=f32) for p, e in zip(fars, es)]
+            row = lax.broadcasted_iota(jnp.int32, (8, 2 * Q_BLOCK), 0)
+            for u in range(group):
+                help_out[k, u] = outs[u][:HEAD_DIM].astype(bf16)
+                help_stat[k, u] = jnp.where(row == 0, outs[u][HEAD_DIM : HEAD_DIM + 1], tops[u])
+            for n in range(2):
+                help_answer(k, n).start()
+
+        pl.when(z == last - 1)(go)
 
     def near(k, some, carry):
         row = lax.broadcasted_iota(jnp.int32, (Q_BLOCK, 2 * Q_BLOCK), 0)
@@ -612,19 +672,23 @@
             if dx:
                 wait_side(dz, dx, k)
         lax.fori_loop(0, q_blocks // unroll, functools.partial(near, k), 0)
+        if k > 0 and far_moves:
+            answer(k - 1)
         for dz in range(2, last):
             relay(dz, k)
 
     def wait_far(piece, k):
         if not far_moves:
             return
-        at = piece_at(piece, k)
+        at = piece_at(piece)
+        own_piece = isinstance(piece, int) and piece == ranks - 1
 
         def wait(first, count):
             region = sel.at[pl.ds(first, count), k, at]
             remote(region, region, x_send.at[0], far_recv.at[k, piece], above).wait_recv()
 
-        pl.when(z == last)(lambda: wait(slot(2, 0), (planes - 2) * across))
+        if not own_piece:
+            pl.when(z == last)(lambda: wait(slot(2, 0), (planes - 2) * across))
         if across > 1:
             for dz in range(2, last):
                 pl.when(z == dz)(lambda: wait(slot(2, 1), across - 1))
@@ -690,11 +754,28 @@
                 jnp.dot(values_of(parts), e, preferred_element_type=f32) for (parts, _), e in zip(fars, es)
             ]
             outs = [o * jnp.exp(a - b) + m for o, a, b, m in zip(outs, old, new, more)]
-        for at, out in zip(ats, outs):
-            o = out[:HEAD_DIM] / out[HEAD_DIM : HEAD_DIM + 1]
+        settle(k, ats, [(out[:HEAD_DIM], out[HEAD_DIM : HEAD_DIM + 1]) for out in outs])
+
+    def settle(k, ats, outs):
+        for at, (value, total) in zip(ats, outs):
+            o = value / total
             o = [o[:, n * Q_BLOCK : (n + 1) * Q_BLOCK] * gate_row(1, 2 * k + n, at) for n in range(2)]
             turned = oc[k, :, at] + jnp.concatenate(o, axis=0)
             mix[k, at, :] = turned.T.astype(bf16)
+
+    def answered(k):
+        for n in range(2):
+            help_answer(k, n).wait_recv()
+        ats, outs = [], []
+        for u in range(group):
+            j = rank * group + u
+            out, top, more, stat = part_out[k, j], part_top[k, j], got_out[k, u].astype(f32), got_stat[k, u]
+            both = jnp.maximum(top, stat[1:2])
+            a, b = jnp.exp(top - both), jnp.exp(stat[1:2] - both)
+            total = out[HEAD_DIM : HEAD_DIM + 1] * a + stat[0:1] * b
+            ats.append(pl.ds(pl.multiple_of(j * Q_BLOCK, Q_BLOCK), Q_BLOCK))
+            outs.append((out[:HEAD_DIM] * a + more * b, total))
+        settle(k, ats, outs)
 
     def choose(k, step, carry):
         pl.when((step > 0) & (step < ranks - 2))(lambda: mix_copy(k, step - 1).start())
@@ -706,20 +787,26 @@
         lax.fori_loop(0, ranks - 2, functools.partial(choose, k), 0)
         if ranks > 2:
             mix_copy(k, ranks - 3).start()
+        if k == 0 and far_moves:
+            answer(kv_local - 1)
         if k > 0:
             add_head(k - 1)
         lax.fori_loop(ranks - 2, ranks - 1, functools.partial(choose, k), 0)
         mix_copy(k, ranks - 2).start()
-        size = group // parts_last[k]
-        for n in range(parts_last[k]):
-            wait_far(ranks - 1 + n, k)
-            mine = [n * size + u for u in range(size)]
-            late(k, [rank * group + u for u in mine])
-            if k == kv_local - 1:
-                if n == 0:
-                    every_mix(k).wait_recv()
-                at, more = outputs(k, n * size, size)
-                out_ref[at, :] = (more if k == 0 else acc[at, :] + more).astype(bf16)
+        def mine(k=k):
+            wait_far(ranks - 1, k)
+            late(k, [rank * group + u for u in range(group)])
+
+        if far_moves:
+            pl.when(z == last)(functools.partial(answered, k))
+            pl.when(z < last)(mine)
+        else:
+            mine()
+    every_mix(kv_local - 1).wait_recv()
+    two = 2 if group % 2 == 0 else 1
+    for n in range(0, group, two):
+        at, more = outputs(kv_local - 1, n, two)
+        out_ref[at, :] = (more if kv_local == 1 else acc[at, :] + more).astype(bf16)
 
 
     for k in range(kv_local):
@@ -738,9 +825,14 @@
         if dz + 1 < last:
             pl.when(whole & (z + 1 < last))(lambda dz=dz, k=k: up_copy(dz, k).wait_send())
         if k == 0 and dz + 1 <= last:
-            pl.when(whole & (z + 1 == last))(
-                lambda dz=dz: sent(stage_t.at[dz - 1], t_send.at[dz - 1]).wait_send()
-            )
+
+            def sent_top(dz=dz):
+                most = pl.ds(0, q_blocks - group)
+                sent(stage_t.at[dz - 1, 0, :, most], t_send.at[dz - 1, 0]).wait_send()
+                if across > 1:
+                    sent(stage_t.at[dz - 1, pl.ds(1, across - 1)], t_send.at[dz - 1, 1]).wait_send()
+
+            pl.when(whole & (z + 1 == last))(sent_top)
         if k == 0 and across > 1:
             pl.when(whole)(lambda dz=dz: sent(stage_x.at[dz], x_send.at[dz]).wait_send())
     for dz in range(1, planes):
@@ -751,6 +843,11 @@
             pl.when(z >= dz)(lambda dz=dz, dx=dx: sum_side(dz, dx, me - dz * across).wait_send())
     for k in range(kv_local):
         every_mix(k).wait_send()
+        if far_moves:
+            for n in range(2):
+                pl.when(z == last - 1)(lambda k=k, n=n: help_answer(k, n).wait_send())
+    if far_moves:
+        pl.when(z == last)(lambda: help_queries().wait_send())
 
 
 def position_tables(rows, owners):
@@ -824,7 +921,8 @@
     n_local = 3 + len(weights) + 8 + 2 + 2
     picks = (owners * kv_local, chosen.shape[1])
     down = max(planes - 2, 1)
-    n_pieces = ranks + 1
+    n_pieces = ranks
+    group = rank_rows // Q_BLOCK
     return pl.pallas_call(
         functools.partial(layer_kernel, planes, len(weights)),
         in_specs=[hbm] * len(operands),
@@ -846,6 +944,12 @@
             pltpu.VMEM((kv_local, q_blocks, 1, 2 * Q_BLOCK), f32),
             pltpu.VMEM((max(planes - 1, 1), max(across - 1, 1), kv_local, *picked), bf16),
             pltpu.VMEM((down, across, kv_local, *picked), bf16),
+            pltpu.VMEM((kv_local, 2, LANES, rank_rows), bf16),
+            pltpu.VMEM((down, max(across - 1, 1), kv_local, group, SEL_BLOCK, LANES), bf16),
+            pltpu.VMEM((kv_local, group, HEAD_DIM, 2 * Q_BLOCK), bf16),
+            pltpu.VMEM((kv_local, group, 8, 2 * Q_BLOCK), f32),
+            pltpu.VMEM((kv_local, group, HEAD_DIM, 2 * Q_BLOCK), bf16),
+            pltpu.VMEM((kv_local, group, 8, 2 * Q_BLOCK), f32),
             pltpu.VMEM((min(3, rows // TILE), TILE, width), bf16),
             pltpu.VMEM(tokens.shape, bf16),
             pltpu.VMEM((width, 4 * kv_width), bf16),
@@ -874,13 +978,18 @@
             dma((kv_local, down)),
             dma((kv_local, max(planes - 1, 1))),
             dma((planes + across,)),
-            dma((down,)),
+            dma((down, 2)),
             dma((max(2 * across - 1, 1), kv_local)),
             dma((kv_local, n_pieces)),
             dma((across, planes)),
             dma((across, planes)),
             dma((kv_local,)),
             dma((kv_local,)),
+            dma((1,)),
+            dma((1,)),
+            dma((kv_local,)),
+            dma((kv_local, 2)),
+            dma((kv_local, 2)),
         ]
         + [pltpu.VMEM(whole, bf16)] * (kv_local * max(planes - 1, 1)),
         compiler_params=pltpu.CompilerParams(

time: 81.3 us -> 77.1 us (0.948); the launches traced: 80 us -> 76.9 us
  Pallas kernels: 78.7 us -> 75.6 us
    pallas_call x1, Pallas kernels: 78.7 us -> 75.6 us  [per_device(): pl.pallas_call(functools.partial(layer_kernel, planes, len(weights)), in_...]
where the time goes in v5:
time: 77.1 us; the launch traced here: 76.9 us
  Pallas kernels  75.6 us (98%)
  local copies, waits for them, and re-layouts  1.32 us (2%)
    pallas_call x1, Pallas kernels, per_device(): pl.pallas_call(functools.partial(layer_kernel, planes, len(weights)), in_...  75.6 us

profile of v5, /device:TPU:27, one launch (start us, length us, event | category | flops | bytes accessed | tf_op | source)
XLA Modules:
  0.0 76.9 jit_solution(2937173839366056685)
XLA Ops:
  0.0 75.6 %layer.1 = bf16[512,2048]{1,0:T(8,128)(2,1)S(1)} custom-call(s32[2,8,128]{2,1,0:T(8,128)} %bitcast.8, bf16[16,128]{1,0:T(8,128)(2,1)} %bitcast.9, bf16[2,32,64]{2,1,0:T(8,128)(2,1)} %refs_2_.1, bf16[2,64,64]{2,1,0:T(8,128)(2,1)} %refs_3_.1, bf16[2,32,64]{2,1,0:T(8,128)(2,1)} %refs_4_.1, bf16[2,64,64]{2,1,0:T(8,128)(2,1)} %refs_5_.1, ...), custom_call_target="tpu_custom_call" | custom-call | flops 30000001024 | bytes 20000000 | tf_op jit(solution)/shard_map/layer/pallas_call | solution.py:926
  75.6 1.3 %copy.20 = bf16[512,2048]{1,0:T(8,128)(2,1)} copy(bf16[512,2048]{1,0:T(8,128)(2,1)S(1)} %layer.1) | data formatting | bytes 4194304

commit v6 on v5

--- a/solution.py
+++ b/solution.py
@@ -635,7 +635,7 @@
             tops = [jnp.max(s, axis=0, keepdims=True) for s in ss]
             es = [jnp.exp(s - t).astype(bf16) for s, t in zip(ss, tops)]
             outs = [jnp.dot(values_of(p), e, preferred_element_type=f32) for p, e in zip(fars, es)]
-            row = lax.broadcasted_iota(jnp.int32, (8, 2 * Q_BLOCK), 0)
+            row = lax.broadcasted_iota(jnp.int32, (2, 2 * Q_BLOCK), 0)
             for u in range(group):
                 help_out[k, u] = outs[u][:HEAD_DIM].astype(bf16)
                 help_stat[k, u] = jnp.where(row == 0, outs[u][HEAD_DIM : HEAD_DIM + 1], tops[u])
@@ -947,9 +947,9 @@
             pltpu.VMEM((kv_local, 2, LANES, rank_rows), bf16),
             pltpu.VMEM((down, max(across - 1, 1), kv_local, group, SEL_BLOCK, LANES), bf16),
             pltpu.VMEM((kv_local, group, HEAD_DIM, 2 * Q_BLOCK), bf16),
-            pltpu.VMEM((kv_local, group, 8, 2 * Q_BLOCK), f32),
+            pltpu.VMEM((kv_local, group, 2, 2 * Q_BLOCK), f32),
             pltpu.VMEM((kv_local, group, HEAD_DIM, 2 * Q_BLOCK), bf16),
-            pltpu.VMEM((kv_local, group, 8, 2 * Q_BLOCK), f32),
+            pltpu.VMEM((kv_local, group, 2, 2 * Q_BLOCK), f32),
             pltpu.VMEM((min(3, rows // TILE), TILE, width), bf16),
             pltpu.VMEM(tokens.shape, bf16),
             pltpu.VMEM((width, 4 * kv_width), bf16),

time: 77.1 us -> 77.6 us (level)
  no operation moved by 1% of the time
where the time goes in v6:
time: 77.6 us; the launch traced here: 77.4 us
  Pallas kernels  76.1 us (98%)
  local copies, waits for them, and re-layouts  1.32 us (2%)
    pallas_call x1, Pallas kernels, per_device(): pl.pallas_call(functools.partial(layer_kernel, planes, len(weights)), in_...  76.1 us

profile of v6, /device:TPU:27, one launch (start us, length us, event | category | flops | bytes accessed | tf_op | source)
XLA Modules:
  0.0 77.4 jit_solution(10063171757275684852)
XLA Ops:
  0.0 76.1 %layer.1 = bf16[512,2048]{1,0:T(8,128)(2,1)S(1)} custom-call(s32[2,8,128]{2,1,0:T(8,128)} %bitcast.8, bf16[16,128]{1,0:T(8,128)(2,1)} %bitcast.9, bf16[2,32,64]{2,1,0:T(8,128)(2,1)} %refs_2_.1, bf16[2,64,64]{2,1,0:T(8,128)(2,1)} %refs_3_.1, bf16[2,32,64]{2,1,0:T(8,128)(2,1)} %refs_4_.1, bf16[2,64,64]{2,1,0:T(8,128)(2,1)} %refs_5_.1, ...), custom_call_target="tpu_custom_call" | custom-call | flops 30000001024 | bytes 20000000 | tf_op jit(solution)/shard_map/layer/pallas_call | solution.py:926
  76.1 1.3 %copy.20 = bf16[512,2048]{1,0:T(8,128)(2,1)} copy(bf16[512,2048]{1,0:T(8,128)(2,1)S(1)} %layer.1) | data formatting | bytes 4194304
